TPU v7x, 32 devices: a whole 2x2x4 slice. The times are simulated.
32 devices in a mesh: sp: 16 (over z, y, core), tp: 2 (over x).
Axes of the slice: x: 2, y: 2, z: 4, core: 2. Of those that a mesh axis runs over, the one named last changes fastest.
Arguments:
- pool_input: bfloat16 [4, 128, 8192], P(None, 'tp', 'sp'), may hold values from -8 to 8
- doc_ids: int32 [8192], P('sp'), may hold values from 0 to 3, never falling along the last dimension, each value on 1 to 4096 neighbouring positions
- pool_map: bfloat16 [4, 128, 128], replicated, may hold values from -0.5 to 0.5
- pool_scale: float32 [512], replicated, may hold values from 0.1 to 1.9
- w_out: bfloat16 [512, 2048], replicated, may hold values from -0.25 to 0.25
- residual: bfloat16 [8192, 2048], P(('sp', 'tp')), may hold values from -6 to 6
- mix_gain: float32 [2048], replicated, may hold values from 0.1 to 1.9
- ffn_gain: float32 [2048], replicated, may hold values from 0.1 to 1.9
- out_gain: float32 [2048], replicated, may hold values from 0.1 to 1.9
- expert_ids: int32 [8192, 2], P(('sp', 'tp')), may hold values from 0 to 31, all different within a row; in each aligned block of 256 rows (0 to 255, 256 to 511, ...) at most 32 rows name the same one
- route_logits: float32 [8192, 2], P(('sp', 'tp')), may hold values from -6 to 6
- w_gate: bfloat16 [32, 2048, 1024], P(('sp', 'tp')), may hold values from -0.125 to 0.125
- w_up: bfloat16 [32, 2048, 1024], P(('sp', 'tp')), may hold values from -0.125 to 0.125
- w_down: bfloat16 [32, 1024, 2048], P(('sp', 'tp')), may hold values from -0.1875 to 0.1875
Outputs:
- layer_out: bfloat16 [8192, 2048], P(('sp', 'tp'))
Inputs may be any that keep to these rules, and one draw needn't show every extreme that they name: `doc_ids`: document numbers never fall along the positions; no document has more than 4096 positions. `expert_ids`: each row names 2 different experts; within each aligned block of 256 rows no expert is named by more than 32 rows, a bound that some block reaches.
All inputs are finite; a program needn't handle non-finite values.
Results may differ from a plain program's by a relative error of at most 0.03.
Values may be sent and summed in bfloat16 or wider, within the bound.
A program may use at most 64 MiB of HBM per device.

v0:
```python
import functools
import jax
import jax.numpy as jnp
from jax import lax
from jax.sharding import PartitionSpec as P
from jax.experimental import pallas as pl
from jax.experimental.pallas import tpu as pltpu

MESH = pl.DeviceIdType.MESH
EPS = 1e-06


def rms_scale(vector):
    return lax.rsqrt(jnp.mean(vector * vector, axis=-1, keepdims=True) + EPS)


def mixer_kernel(
    sp_count, tp_count,
    pool_ref, doc_ref, map_ref, scale_ref, w_out_ref, residual_ref, mix_ref, ffn_ref,
    stream_ref, normed_ref,
    tail_out, tails, run_out, far, diff_out, parts,
    tail_send, tail_recv, far_send, far_recv, diff_send, diff_recv,
):
    groups, channels, length = pool_ref.shape
    rows = length // tp_count
    lines = groups * channels
    sp, tp = lax.axis_index("sp"), lax.axis_index("tp")

    barrier = pltpu.get_barrier_semaphore()
    for i in range(1, sp_count):
        pl.semaphore_signal(
            barrier, inc=1, device_id=(lax.rem(sp + i, sp_count), tp), device_id_type=MESH
        )
    for i in range(1, tp_count):
        pl.semaphore_signal(
            barrier, inc=1, device_id=(sp, lax.rem(tp + i, tp_count)), device_id_type=MESH
        )

    values = pool_ref[...].reshape(lines, length)
    doc = doc_ref[...].astype(jnp.float32)
    last_id = doc[:, length - 1 :]
    tail_mask = jnp.broadcast_to((doc == last_id).astype(jnp.bfloat16), (8, length))
    tail_sum = lax.dot_general(
        tail_mask, values, (((1,), (1,)), ((), ())), preferred_element_type=jnp.float32
    )[:1]
    tail_count = jnp.sum((doc == last_id).astype(jnp.float32), axis=1, keepdims=True)
    tail_row = jnp.concatenate(
        [
            tail_sum,
            jnp.broadcast_to(last_id, (1, 128)),
            jnp.broadcast_to(tail_count, (1, 128)),
        ],
        axis=1,
    )
    tail_out[...] = tail_row
    tails[sp] = tail_row
    pl.semaphore_wait(barrier, sp_count + tp_count - 2)
    tail_copies = []
    for i in range(1, sp_count):
        copy = pltpu.make_async_remote_copy(
            src_ref=tail_out,
            dst_ref=tails.at[sp],
            send_sem=tail_send.at[i],
            recv_sem=tail_recv.at[i],
            device_id=(lax.rem(sp + i, sp_count), tp),
            device_id_type=MESH,
        )
        copy.start()
        tail_copies.append(copy)

    doc_col = jnp.broadcast_to(doc, (128, length)).T[:, :1]
    row_at = lax.broadcasted_iota(jnp.int32, (length, length), 0)
    col_at = lax.broadcasted_iota(jnp.int32, (length, length), 1)
    same = jnp.where((row_at <= col_at) & (doc_col == doc), 1.0, 0.0)
    local_count = jnp.sum(same, axis=0, keepdims=True)
    local_run = jnp.dot(values, same.astype(jnp.bfloat16), preferred_element_type=jnp.float32)

    for copy in tail_copies:
        copy.wait()
    table = jnp.concatenate([tails[j] for j in range(sp_count)], axis=0)
    sources = lax.broadcasted_iota(jnp.int32, (sp_count, 1), 0)
    joined = jnp.where(
        (sources < sp) & (table[:, lines : lines + 1] == doc), 1.0, 0.0
    )
    running = local_run + lax.dot_general(
        table[:, :lines],
        joined,
        (((0,), (0,)), ((), ())),
        preferred_element_type=jnp.float32,
        precision=lax.Precision.HIGHEST,
    )
    position = local_count + jnp.sum(
        joined * table[:, lines + 128 : lines + 129], axis=0, keepdims=True
    )
    run_out[...] = running.astype(jnp.bfloat16).reshape(groups, channels, length)
    far_copies = []
    for g in reversed(range(groups)):
        copy = pltpu.make_async_remote_copy(
            src_ref=run_out.at[g],
            dst_ref=far.at[g],
            send_sem=far_send.at[g],
            recv_sem=far_recv.at[g],
            device_id=(lax.rem(sp + 2**g, sp_count), tp),
            device_id_type=MESH,
        )
        copy.start()
        far_copies.append(copy)
    for copy in far_copies:
        copy.wait()
    for g in range(groups):
        span = float(length * 2**g)
        at = slice(g * channels, (g + 1) * channels)
        window = running[at] - jnp.where(position > span, far[g].astype(jnp.float32), 0.0)
        diff = window / jnp.minimum(position, span) - values[at].astype(jnp.float32)
        diff = diff.astype(jnp.bfloat16)
        for q in range(tp_count):
            diff_out[q, g] = diff[:, q * rows : (q + 1) * rows]
    parts[tp] = diff_out[tp]
    diff_copies = []
    for i in range(1, tp_count):
        other = lax.rem(tp + i, tp_count)
        copy = pltpu.make_async_remote_copy(
            src_ref=diff_out.at[other],
            dst_ref=parts.at[tp],
            send_sem=diff_send.at[i],
            recv_sem=diff_recv.at[i],
            device_id=(sp, other),
            device_id_type=MESH,
        )
        copy.start()
        diff_copies.append(copy)
    for copy in diff_copies:
        copy.wait()
    mapped = []
    for g in range(groups):
        channel_rows = jnp.concatenate([parts[q, g] for q in range(tp_count)], axis=0)
        mapped.append(
            lax.dot_general(
                channel_rows,
                map_ref[g],
                (((0,), (0,)), ((), ())),
                preferred_element_type=jnp.float32,
            )
        )
    mapped = (jnp.concatenate(mapped, axis=1) * scale_ref[...]).astype(jnp.bfloat16)
    projected = jnp.dot(mapped, w_out_ref[...], preferred_element_type=jnp.float32)
    stream = (
        residual_ref[...].astype(jnp.float32) + mix_ref[...] * projected * rms_scale(projected)
    ).astype(jnp.bfloat16)
    stream_ref[...] = stream
    back = stream.astype(jnp.float32)
    normed_ref[...] = (ffn_ref[...] * back * rms_scale(back)).astype(jnp.bfloat16)


def mixer(pool_input, doc_ids, pool_map, pool_scale, w_out, residual, mix_gain, ffn_gain):
    groups, channels, length = pool_input.shape
    sp_count, tp_count = lax.axis_size("sp"), lax.axis_size("tp")
    rows = length // tp_count
    tail_width = groups * channels + 256
    vmem = pl.BlockSpec(memory_space=pltpu.VMEM)
    shape = jax.ShapeDtypeStruct(residual.shape, jnp.bfloat16)
    return pl.pallas_call(
        functools.partial(mixer_kernel, sp_count, tp_count),
        out_shape=(shape, shape),
        in_specs=[vmem] * 8,
        out_specs=(vmem, vmem),
        scratch_shapes=[
            pltpu.VMEM((1, tail_width), jnp.float32),
            pltpu.VMEM((sp_count, 1, tail_width), jnp.float32),
            pltpu.VMEM((groups, channels, length), jnp.bfloat16),
            pltpu.VMEM((groups, channels, length), jnp.bfloat16),
            pltpu.VMEM((tp_count, groups, channels, rows), jnp.bfloat16),
            pltpu.VMEM((tp_count, groups, channels, rows), jnp.bfloat16),
            pltpu.SemaphoreType.DMA((sp_count,)),
            pltpu.SemaphoreType.DMA((sp_count,)),
            pltpu.SemaphoreType.DMA((groups,)),
            pltpu.SemaphoreType.DMA((groups,)),
            pltpu.SemaphoreType.DMA((tp_count,)),
            pltpu.SemaphoreType.DMA((tp_count,)),
        ],
        compiler_params=pltpu.CompilerParams(collective_id=0, has_side_effects=True),
    )(
        pool_input,
        doc_ids.reshape(1, -1),
        pool_map,
        pool_scale.reshape(1, -1),
        w_out,
        residual,
        mix_gain.reshape(1, -1),
        ffn_gain.reshape(1, -1),
    )


def expert_rows(row_data, w_gate, w_up, w_down):
    gate_act = jnp.dot(row_data, w_gate[0], preferred_element_type=jnp.float32)
    up_act = jnp.dot(row_data, w_up[0], preferred_element_type=jnp.float32)
    hidden = (jax.nn.silu(gate_act) * up_act).astype(jnp.bfloat16)
    return jnp.dot(hidden, w_down[0], preferred_element_type=jnp.float32).astype(jnp.bfloat16)


def slots_of(expert_ids, experts, capacity):
    rows = expert_ids.shape[0]
    ids = jnp.arange(experts, dtype=jnp.int32)
    chosen = (expert_ids[:, :, None] == ids).astype(jnp.float32)
    named = jnp.sum(chosen, axis=1)
    at = jnp.arange(rows)
    earlier = (at[:, None] > at[None, :]).astype(jnp.bfloat16)
    rank = jnp.dot(earlier, named.astype(jnp.bfloat16), preferred_element_type=jnp.float32)
    return expert_ids * capacity + jnp.sum(chosen * rank[:, None, :], axis=2).astype(jnp.int32)


def local(
    pool_input, doc_ids, pool_map, pool_scale, w_out, residual, mix_gain, ffn_gain, out_gain,
    expert_ids, route_logits, w_gate, w_up, w_down,
):
    row_count, top_count = expert_ids.shape
    width = residual.shape[1]
    experts = w_gate.shape[0] * lax.axis_size("sp") * lax.axis_size("tp")
    capacity = max(2, 2 * row_count * top_count // experts)
    slots = slots_of(expert_ids, experts, capacity)
    places = jnp.arange(experts * capacity, dtype=jnp.int32)
    picked = jnp.zeros((experts * capacity, row_count), jnp.bool_)
    for k in range(top_count):
        picked = picked | (places[:, None] == slots[:, k][None, :])
    picked = picked.astype(jnp.bfloat16)
    weights = jax.nn.sigmoid(route_logits - route_logits[:, ::-1])
    mix = jnp.zeros((row_count, experts * capacity), jnp.float32)
    for k in range(top_count):
        mix = mix + jnp.where(slots[:, k : k + 1] == places[None, :], weights[:, k : k + 1], 0.0)
    mix_high = mix.astype(jnp.bfloat16)
    mix_low = (mix - mix_high.astype(jnp.float32)).astype(jnp.bfloat16)

    stream, normed = mixer(
        pool_input, doc_ids, pool_map, pool_scale, w_out, residual, mix_gain, ffn_gain
    )
    outgoing = jnp.dot(picked, normed, preferred_element_type=jnp.float32).astype(jnp.bfloat16)
    outgoing = outgoing.reshape(experts, capacity, width)
    arrived = lax.all_to_all(outgoing, ("sp", "tp"), split_axis=0, concat_axis=0, tiled=True)
    finished = expert_rows(arrived.reshape(-1, width), w_gate, w_up, w_down).reshape(arrived.shape)
    results = lax.all_to_all(
        finished, ("sp", "tp"), split_axis=0, concat_axis=0, tiled=True
    ).reshape(-1, width)
    expert_sum = jnp.dot(mix_high, results, preferred_element_type=jnp.float32)
    expert_sum = expert_sum + jnp.dot(mix_low, results, preferred_element_type=jnp.float32)
    back = stream.astype(jnp.float32)
    return (back + out_gain * expert_sum * rms_scale(expert_sum)).astype(jnp.bfloat16)


def solution(mesh):
    rows = P(("sp", "tp"), None)
    cubes = P(("sp", "tp"), None, None)
    in_specs = (
        P(None, "tp", "sp"), P("sp"), P(), P(), P(), rows, P(), P(), P(), rows, rows,
        cubes, cubes, cubes,
    )
    return jax.shard_map(local, mesh=mesh, in_specs=in_specs, out_specs=rows, check_vma=False)
```

profile of v0, /device:TPU:4, one launch (start us, length us, event | category | flops | bytes accessed | tf_op | source)
XLA Modules:
  0.0 250.3 jit_solution(8108853677316903561)
XLA Ops:
  0.0 0.7 convert_reduce_fusion
  0.7 0.2 fusion.24
  0.8 0.7 select_reduce_fusion
  1.6 0.7 convert_add_fusion
  2.3 27.1 %shard_map.136 = (bf16[256,2048]{1,0:T(8,128)(2,1)}, bf16[256,2048]{1,0:T(8,128)(2,1)}) custom-call(bf16[4,64,512]{2,1,0:T(8,128)(2,1)} %pool_ref.1, s32[1,512]{1,0:T(1,128)} %bitcast.44, bf16[4,128,128]{2,1,0:T(8,128)(2,1)} %map_ref.1, f32[1,512]{1,0:T(1,128)} %bitcast.45, bf16[512,2048]{1,0:T(8,128)(2,1)} %w_out_ref.1, bf16[256,2048]{1,0:T(8,128)(2,1)} %residual_ref.1, ...), custom_call_target="tpu_custom_call" | custom-call | tf_op jit(solution)/shard_map/pallas_call | solution.py:162
  29.4 2.5 convolution_convert_fusion
  31.9 0.0 copy-start.3
  31.9 96.2 %all_to_all.10 = bf16[32,32,2048]{2,1,0:T(8,128)(2,1)S(1)} all-to-all(bf16[32,32,2048]{2,1,0:T(8,128)(2,1)S(1)} %bitcast.32), channel_id=1, replica_groups=mesh['sp'=16,'tp'=2] {'sp','tp'}, dimensions={0} | all-to-all | bytes 8388608 | tf_op jit(solution)/shard_map/all_to_all | solution.py:238
  128.1 0.0 copy-done.3
  128.1 0.0 copy-start.4
  128.1 4.5 %fusion.2 = f32[1024,1024]{1,0:T(8,128)S(1)} fusion(bf16[1024,2048]{1,0:T(8,128)(2,1)S(1)} %bitcast.34, bf16[1,2048,1024]{2,1,0:T(8,128)(2,1)S(1)} %copy-done.3), kind=kOutput, calls=%fused_computation.2 | convolution fusion | flops 4294967296 | bytes 12582912 | tf_op jit(solution)/shard_map/dot_general | solution.py:196
  132.6 0.0 copy-done.4
  132.6 0.0 copy-start.5
  132.6 5.4 %multiply_convert_fusion = bf16[1024,1024]{1,0:T(8,128)(2,1)S(1)} fusion(f32[1024,1024]{1,0:T(8,128)S(1)} %fusion.2, bf16[1024,2048]{1,0:T(8,128)(2,1)S(1)} %bitcast.35, bf16[1,2048,1024]{2,1,0:T(8,128)(2,1)S(1)} %copy-done.4), kind=kOutput, calls=%fused_computation.6 | convolution fusion | flops 4301258752 | bytes 14680064 | tf_op jit(solution)/shard_map/dot_general | solution.py:195
  138.0 0.0 copy-done.5
  138.0 6.1 %fusion.6 = bf16[1024,2048]{1,0:T(8,128)(2,1)} fusion(bf16[1024,1024]{1,0:T(8,128)(2,1)S(1)} %multiply_convert_fusion, bf16[1,1024,2048]{2,1,0:T(8,128)(2,1)S(1)} %copy-done.5), kind=kOutput, calls=%fused_computation.8 | convolution fusion | flops 4297064448 | bytes 10485760 | tf_op jit(solution)/shard_map/dot_general | solution.py:198
  144.1 0.0 copy-start.2
  144.1 3.9 %all-to-all-start.1 = ((bf16[32,32,2048]{2,1,0:T(8,128)(2,1)}), bf16[32,32,2048]{2,1,0:T(8,128)(2,1)}, u32[]{:S(2)}, u32[]{:S(2)}) async-start(bf16[32,32,2048]{2,1,0:T(8,128)(2,1)} %bitcast.33), calls=%async_computation.1 | async-start | bytes 8388608 | tf_op jit(solution)/shard_map/all_to_all | solution.py:240
  148.1 0.0 copy-done.2
  148.1 0.1 rev.3
  148.2 93.2 %all-to-all-done.1 = bf16[32,32,2048]{2,1,0:T(8,128)(2,1)} async-done(((bf16[32,32,2048]{2,1,0:T(8,128)(2,1)}), bf16[32,32,2048]{2,1,0:T(8,128)(2,1)}, u32[]{:S(2)}, u32[]{:S(2)}) %all-to-all-start.1) | async-done | bytes 4194336 | tf_op jit(solution)/shard_map/all_to_all | solution.py:240
  241.4 3.7 %fusion.22 = f32[256,2048]{1,0:T(8,128)S(1)} fusion(bf16[1024,2048]{1,0:T(8,128)(2,1)} %bitcast.14, f32[256]{0:T(256)S(1)} %bitcast.48, s32[256]{0:T(256)S(1)} %bitcast.40, f32[256]{0:T(256)S(1)} %bitcast.46, s32[256]{0:T(256)S(1)} %bitcast.37), kind=kOutput, calls=%fused_computation.27 | convolution fusion | flops 1075314688 | bytes 6295552 | tf_op jit(solution)/shard_map/dot_general | solution.py:243
  245.1 0.0 copy-start
  245.1 0.0 copy-start.1
  245.1 3.9 %multiply_reduce_fusion = (f32[256]{0:T(256)S(1)}, f32[256,2048]{1,0:T(8,128)S(1)}) fusion(f32[256,2048]{1,0:T(8,128)S(1)} %fusion.22, bf16[1024,2048]{1,0:T(8,128)(2,1)} %bitcast.14, f32[256]{0:T(256)S(1)} %bitcast.49, s32[256]{0:T(256)S(1)} %bitcast.41, f32[256]{0:T(256)S(1)} %bitcast.47, s32[256]{0:T(256)S(1)} %bitcast.38), kind=kOutput, calls=%fused_computation.11 | convolution fusion | flops 1077673728 | bytes 8393728 | tf_op jit(solution)/shard_map/dot_general | solution.py:244
  249.0 0.0 copy-done
  249.0 0.0 copy-done.1
  249.0 1.3 add_convert_fusion
  (4 shorter events, 0.0 us)
Async XLA Ops:
  31.9 96.2 %copy-start.3 = (bf16[1,2048,1024]{2,1,0:T(8,128)(2,1)S(1)}, bf16[1,2048,1024]{2,1,0:T(8,128)(2,1)}, u32[]{:S(2)}) copy-start(bf16[1,2048,1024]{2,1,0:T(8,128)(2,1)} %param.26) | copy-start | bytes 12582916
  128.1 4.5 %copy-start.4 = (bf16[1,2048,1024]{2,1,0:T(8,128)(2,1)S(1)}, bf16[1,2048,1024]{2,1,0:T(8,128)(2,1)}, u32[]{:S(2)}) copy-start(bf16[1,2048,1024]{2,1,0:T(8,128)(2,1)} %param.25) | copy-start | bytes 12582916
  132.6 5.4 %copy-start.5 = (bf16[1,1024,2048]{2,1,0:T(8,128)(2,1)S(1)}, bf16[1,1024,2048]{2,1,0:T(8,128)(2,1)}, u32[]{:S(2)}) copy-start(bf16[1,1024,2048]{2,1,0:T(8,128)(2,1)} %param.27) | copy-start | bytes 12582916
  144.1 3.9 %copy-start.2 = (f32[256,2]{0,1:T(2,128)S(1)}, f32[256,2]{0,1:T(2,128)}, u32[]{:S(2)}) copy-start(f32[256,2]{0,1:T(2,128)} %param.24) | copy-start | bytes 6148
  144.1 97.3 %all-to-all-start.1 = ((bf16[32,32,2048]{2,1,0:T(8,128)(2,1)}), bf16[32,32,2048]{2,1,0:T(8,128)(2,1)}, u32[]{:S(2)}, u32[]{:S(2)}) async-start(bf16[32,32,2048]{2,1,0:T(8,128)(2,1)} %bitcast.33), calls=%async_computation.1 | async-start | bytes 8388608 | tf_op jit(solution)/shard_map/all_to_all | solution.py:240
  245.1 3.9 %copy-start = (bf16[256,2048]{1,0:T(8,128)(2,1)S(1)}, bf16[256,2048]{1,0:T(8,128)(2,1)}, u32[]{:S(2)}) copy-start(bf16[256,2048]{1,0:T(8,128)(2,1)} %get-tuple-element.7) | copy-start | bytes 3145732
  245.1 3.9 %copy-start.1 = (f32[2048]{0:T(1024)S(1)}, f32[2048]{0:T(1024)}, u32[]{:S(2)}) copy-start(f32[2048]{0:T(1024)} %param.22) | copy-start | bytes 24580
where the time goes:
time: 252 us; the launch traced here: 250 us
  blocking collectives  96.2 us (38%)
  waiting for transfers between devices  93.2 us (37%)
  Pallas kernels  27.1 us (11%)
  matrix products  26.1 us (10%)
  starting transfers between devices  3.93 us (2%)
  other arithmetic  3.48 us (1%)
    all_to_all x1, blocking collectives, local(): lax.all_to_all(outgoing, ('sp', 'tp'), split_axis=0, concat_axis=0, tiled...  96.2 us
    all_to_all x1, waiting for transfers between devices, local(): lax.all_to_all(finished, ('sp', 'tp'), split_axis=0, concat_axis=0, tiled...  93.2 us
    pallas_call x1, Pallas kernels, mixer(): pl.pallas_call(functools.partial(mixer_kernel, sp_count, tp_count), out_s...  27.1 us
    dot_general x1, matrix products, expert_rows(): jnp.dot(hidden, w_down[0], preferred_element_type=jnp.float32)  6.1 us
    dot_general x1, matrix products, expert_rows(): gate_act = jnp.dot(row_data, w_gate[0], preferred_element_type=jnp.float32)  5.35 us
  transfers between devices with their start and end apart: 1, of which 1 were waited for; matrix products, arithmetic and copies ran while one was open for 0% of the time, Pallas kernels for 0%

commit v1 on v0

v1 whole, which is shorter than its diff:
```python
import functools
import jax
import jax.numpy as jnp
from jax import lax
from jax.sharding import PartitionSpec as P
from jax.experimental import pallas as pl
from jax.experimental.pallas import tpu as pltpu

MESH = pl.DeviceIdType.MESH
EPS = 1e-06
CHUNKS = 4
PIECES = 4
F32 = jnp.float32
BF16 = jnp.bfloat16


def rms_scale(vector):
    return lax.rsqrt(jnp.mean(vector * vector, axis=-1, keepdims=True) + EPS)


def contract(left, right, left_dim, right_dim, **options):
    return lax.dot_general(
        left, right, (((left_dim,), (right_dim,)), ((), ())), preferred_element_type=F32, **options
    )


def layer_kernel(
    sp_count, tp_count,
    pool_ref, doc_ref, map_ref, scale_ref, mix_ref, ffn_ref, gain_ref, ids_ref, logits_ref,
    residual_hbm, w_out_hbm, w_gate_hbm, w_up_hbm, w_down_hbm,
    out_ref,
    tail_out, tails, run_out, far, diff_out, parts,
    resid, resid_far, mapped_own, mapped_far, ids_far, logits_far,
    w_out, w_gate, w_up, w_down,
    stream, normed, picked, mix_high, mix_low,
    outgoing, arrived, hidden, finished, results, total, partial_out, partial_in,
    load_sem, tail_send, tail_recv, far_send, far_recv, diff_send, diff_recv,
    mirror_send, mirror_recv, out_send, out_recv, back_send, back_recv, part_send, part_recv,
):
    groups, channels, length = pool_ref.shape
    rows = length // tp_count
    lines = groups * channels
    chunks, _, wide = normed.shape
    peers, capacity = outgoing.shape[2], outgoing.shape[3]
    slots = peers * capacity
    tile, depth = hidden.shape[2], hidden.shape[0]
    sp, tp = lax.axis_index("sp"), lax.axis_index("tp")
    half_count = sp_count // 2
    half = sp // half_count
    me = (sp - half * half_count) * tp_count + tp
    mirror = (lax.rem(sp + half_count, sp_count), tp)

    loads = []
    for i, (source, target) in enumerate((
        (residual_hbm, resid), (w_out_hbm, w_out), (w_gate_hbm.at[0], w_gate),
        (w_up_hbm.at[0], w_up), (w_down_hbm.at[0], w_down),
    )):
        copy = pltpu.make_async_copy(source, target, load_sem.at[i])
        copy.start()
        loads.append(copy)

    barrier = pltpu.get_barrier_semaphore()
    for i in range(1, sp_count):
        pl.semaphore_signal(
            barrier, inc=1, device_id=(lax.rem(sp + i, sp_count), tp), device_id_type=MESH
        )
    for j in range(half_count):
        for i in range(1, tp_count):
            pl.semaphore_signal(
                barrier, inc=1,
                device_id=(half * half_count + j, lax.rem(tp + i, tp_count)),
                device_id_type=MESH,
            )

    values = pool_ref[...].reshape(lines, length)
    doc = doc_ref[...].astype(F32)
    last_id = doc[:, length - 1 :]
    tail_mask = jnp.broadcast_to((doc == last_id).astype(BF16), (8, length))
    tail_sum = contract(tail_mask, values, 1, 1)[:1]
    tail_count = jnp.sum((doc == last_id).astype(F32), axis=1, keepdims=True)
    tail_row = jnp.concatenate(
        [
            tail_sum,
            jnp.broadcast_to(last_id, (1, 128)),
            jnp.broadcast_to(tail_count, (1, 128)),
        ],
        axis=1,
    )
    tail_out[...] = tail_row
    tails[sp] = tail_row
    pl.semaphore_wait(barrier, sp_count - 1 + half_count * (tp_count - 1))
    tail_copies = []
    for i in range(1, sp_count):
        copy = pltpu.make_async_remote_copy(
            src_ref=tail_out,
            dst_ref=tails.at[sp],
            send_sem=tail_send.at[i],
            recv_sem=tail_recv.at[i],
            device_id=(lax.rem(sp + i, sp_count), tp),
            device_id_type=MESH,
        )
        copy.start()
        tail_copies.append(copy)

    mirror_copies = []

    def to_mirror(source, target):
        i = len(mirror_copies)
        copy = pltpu.make_async_remote_copy(
            src_ref=source,
            dst_ref=target,
            send_sem=mirror_send.at[i],
            recv_sem=mirror_recv.at[i],
            device_id=mirror,
            device_id_type=MESH,
        )
        copy.start()
        mirror_copies.append(copy)

    to_mirror(ids_ref, ids_far)
    to_mirror(logits_ref, logits_far)
    loads[0].wait()
    piece = rows // PIECES
    to_mirror(resid.at[pl.ds(0, piece)], resid_far.at[pl.ds(0, piece)])

    doc_col = jnp.broadcast_to(doc, (128, length)).T[:, :1]
    row_at = lax.broadcasted_iota(jnp.int32, (length, length), 0)
    col_at = lax.broadcasted_iota(jnp.int32, (length, length), 1)
    same = jnp.where((row_at <= col_at) & (doc_col == doc), 1.0, 0.0)
    local_count = jnp.sum(same, axis=0, keepdims=True)
    local_run = jnp.dot(values, same.astype(BF16), preferred_element_type=F32)

    for copy in tail_copies:
        copy.wait()
    table = jnp.concatenate([tails[j] for j in range(sp_count)], axis=0)
    sources = lax.broadcasted_iota(jnp.int32, (sp_count, 1), 0)
    joined = jnp.where((sources < sp) & (table[:, lines : lines + 1] == doc), 1.0, 0.0)
    running = local_run + contract(
        table[:, :lines], joined, 0, 0, precision=lax.Precision.HIGHEST
    )
    position = local_count + jnp.sum(
        joined * table[:, lines + 128 : lines + 129], axis=0, keepdims=True
    )
    run_out[...] = running.astype(BF16).reshape(groups, channels, length)
    far_copies = []
    for g in reversed(range(groups)):
        copy = pltpu.make_async_remote_copy(
            src_ref=run_out.at[g],
            dst_ref=far.at[g],
            send_sem=far_send.at[g],
            recv_sem=far_recv.at[g],
            device_id=(lax.rem(sp + 2**g, sp_count), tp),
            device_id_type=MESH,
        )
        copy.start()
        far_copies.append(copy)
    for i in range(1, PIECES):
        at = pl.ds(i * piece, piece)
        to_mirror(resid.at[at], resid_far.at[at])

    expand = (
        lax.broadcasted_iota(jnp.int32, (slots, peers), 0) // capacity
        == lax.broadcasted_iota(jnp.int32, (slots, peers), 1)
    ).astype(BF16)
    at_row = lax.broadcasted_iota(jnp.int32, (rows, rows), 0)
    at_col = lax.broadcasted_iota(jnp.int32, (rows, rows), 1)
    earlier = (at_row < at_col).astype(BF16)
    slot_down = lax.rem(lax.broadcasted_iota(jnp.int32, (slots, rows), 0), capacity).astype(F32)
    slot_across = lax.rem(lax.broadcasted_iota(jnp.int32, (rows, slots), 1), capacity).astype(F32)
    experts = lax.broadcasted_iota(jnp.int32, (peers, rows), 0) + half * peers

    def place(block, ids, logits):
        first, second = ids[0:1] == experts, ids[1:2] == experts
        named = jnp.where(first | second, 1.0, 0.0)
        rank = jnp.dot(named.astype(BF16), earlier, preferred_element_type=F32)
        code = jnp.where(named > 0.0, rank, -1.0).astype(BF16)
        picked[block] = jnp.where(
            jnp.dot(expand, code, preferred_element_type=F32) == slot_down, 1.0, 0.0
        ).astype(BF16)
        weight = jnp.where(first, jax.nn.sigmoid(logits[0:1] - logits[1:2]), 0.0) + jnp.where(
            second, jax.nn.sigmoid(logits[1:2] - logits[0:1]), 0.0
        )
        high = weight.astype(BF16)
        low = (weight - high.astype(F32)).astype(BF16)
        here = contract(code, expand, 0, 1) == slot_across
        mix_high[block] = jnp.where(here, contract(high, expand, 0, 1), 0.0).astype(BF16)
        mix_low[block] = jnp.where(here, contract(low, expand, 0, 1), 0.0).astype(BF16)

    place(0, ids_ref[...], logits_ref[...])

    for copy in far_copies:
        copy.wait()
    for g in range(groups):
        span = float(length * 2**g)
        at = slice(g * channels, (g + 1) * channels)
        window = running[at] - jnp.where(position > span, far[g].astype(F32), 0.0)
        diff = window / jnp.minimum(position, span) - values[at].astype(F32)
        diff = diff.astype(BF16)
        for q in range(tp_count):
            diff_out[q, g] = diff[:, q * rows : (q + 1) * rows]
    parts[tp] = diff_out[tp]
    diff_copies = []
    for i in range(1, tp_count):
        other = lax.rem(tp + i, tp_count)
        copy = pltpu.make_async_remote_copy(
            src_ref=diff_out.at[other],
            dst_ref=parts.at[tp],
            send_sem=diff_send.at[i],
            recv_sem=diff_recv.at[i],
            device_id=(sp, other),
            device_id_type=MESH,
        )
        copy.start()
        diff_copies.append(copy)
    for copy in diff_copies:
        copy.wait()
    for g in range(groups):
        channel_rows = jnp.concatenate([parts[q, g] for q in range(tp_count)], axis=0)
        size = tp_count * channels
        at = slice(g * size, (g + 1) * size)
        mapped_own[:, at] = (contract(channel_rows, map_ref[g], 0, 0) * scale_ref[:, at]).astype(BF16)
    to_mirror(mapped_own, mapped_far)
    loads[1].wait()

    step = min(rows, 128)

    def norm_rows(mapped_ref, resid_ref, keep):
        def body(i, carry):
            at = pl.ds(pl.multiple_of(i * step, step), step)
            projected = jnp.dot(mapped_ref[at, :], w_out[...], preferred_element_type=F32)
            line = (
                resid_ref[at, :].astype(F32) + mix_ref[...] * projected * rms_scale(projected)
            ).astype(BF16)
            if keep:
                stream[at, :] = line
            back = line.astype(F32)
            ready = (ffn_ref[...] * back * rms_scale(back)).astype(BF16)
            for c in range(chunks):
                normed[c, at, :] = ready[:, c * wide : (c + 1) * wide]
            return carry

        lax.fori_loop(0, rows // step, body, 0)

    def spread(source, target, send, recv, block, c):
        def body(i, carry):
            peer = lax.rem(me + i, peers)
            place_sp = half * half_count + peer // tp_count
            pltpu.make_async_remote_copy(
                src_ref=source.at[block, c, peer],
                dst_ref=target.at[block, c, me],
                send_sem=send.at[block, c],
                recv_sem=recv.at[block, c],
                device_id=(place_sp, lax.rem(peer, tp_count)),
                device_id_type=MESH,
            ).start()
            return carry

        lax.fori_loop(1, peers, body, 0)
        target[block, c, me] = source[block, c, me]

    def settle(buffer, sem, block, c):
        whole = buffer.at[block, c, pl.ds(0, peers - 1)]
        pltpu.make_async_copy(whole, whole, sem.at[block, c]).wait()

    def hand_out(block):
        def body(c, carry):
            packed = jnp.dot(picked[block], normed[c], preferred_element_type=F32)
            outgoing[block, c] = packed.astype(BF16).reshape(peers, capacity, wide)
            spread(outgoing, arrived, out_send, out_recv, block, c)
            return carry

        lax.fori_loop(0, chunks, body, 0)

    def expert_in(block):
        def body(f, carry):
            at = pl.ds(pl.multiple_of(f * tile, tile), tile)
            gate = jnp.zeros((slots, tile), F32)
            up = jnp.zeros((slots, tile), F32)
            for c in range(chunks):
                line = arrived[block, c].reshape(slots, wide)
                inner = slice(c * wide, (c + 1) * wide)
                gate = gate + jnp.dot(line, w_gate[inner, at], preferred_element_type=F32)
                up = up + jnp.dot(line, w_up[inner, at], preferred_element_type=F32)
            hidden[f] = (jax.nn.silu(gate) * up).astype(BF16)
            return carry

        lax.fori_loop(0, depth, body, 0)

    def expert_out(block, then):
        def body(c, carry):
            at = pl.ds(pl.multiple_of(c * wide, wide), wide)
            value = jnp.zeros((slots, wide), F32)
            for f in range(depth):
                inner = slice(f * tile, (f + 1) * tile)
                value = value + jnp.dot(hidden[f], w_down[inner, at], preferred_element_type=F32)
            finished[block, c] = value.astype(BF16).reshape(peers, capacity, wide)
            if then:
                spread(finished, results, back_send, back_recv, block, c)
            return carry

        lax.fori_loop(0, chunks, body, 0)

    def gathered(block, c):
        line = results[block, c].reshape(slots, wide)
        return jnp.dot(mix_high[block], line, preferred_element_type=F32) + jnp.dot(
            mix_low[block], line, preferred_element_type=F32
        )

    norm_rows(mapped_own, resid, True)
    hand_out(0)
    for copy in mirror_copies[:2]:
        copy.wait()
    place(1, ids_far[...], logits_far[...])
    for copy in mirror_copies[2:]:
        copy.wait()
    norm_rows(mapped_far, resid_far, False)
    hand_out(1)

    for copy in loads[2:]:
        copy.wait()
    for c in range(chunks):
        settle(arrived, out_recv, 0, c)
    expert_in(0)
    expert_out(0, False)
    for c in range(chunks):
        settle(arrived, out_recv, 1, c)
    expert_in(1)
    expert_out(1, True)
    for c in range(chunks):
        spread(finished, results, back_send, back_recv, 0, c)
    part_copies = []
    for c in range(chunks):
        settle(results, back_recv, 1, c)
        partial_out[c] = gathered(1, c).astype(BF16)
        copy = pltpu.make_async_remote_copy(
            src_ref=partial_out.at[c],
            dst_ref=partial_in.at[c],
            send_sem=part_send.at[c],
            recv_sem=part_recv.at[c],
            device_id=mirror,
            device_id_type=MESH,
        )
        copy.start()
        part_copies.append(copy)
    for c in range(chunks):
        settle(results, back_recv, 0, c)
        total[c] = gathered(0, c)
    for block in range(2):
        for c in range(chunks):
            settle(outgoing, out_send, block, c)
            settle(finished, back_send, block, c)
    for copy in part_copies:
        copy.wait()

    def finish(i, carry):
        at = pl.ds(pl.multiple_of(i * step, step), step)
        summed = jnp.concatenate(
            [total[c, at, :] + partial_in[c, at, :].astype(F32) for c in range(chunks)], axis=1
        )
        out_ref[at, :] = (
            stream[at, :].astype(F32) + gain_ref[...] * summed * rms_scale(summed)
        ).astype(BF16)
        return carry

    lax.fori_loop(0, rows // step, finish, 0)


def local(
    pool_input, doc_ids, pool_map, pool_scale, w_out, residual, mix_gain, ffn_gain, out_gain,
    expert_ids, route_logits, w_gate, w_up, w_down,
):
    groups, channels, length = pool_input.shape
    sp_count, tp_count = lax.axis_size("sp"), lax.axis_size("tp")
    rows, top_count = expert_ids.shape
    width, hidden_width = w_gate.shape[1], w_gate.shape[2]
    experts = sp_count * tp_count
    peers = experts // 2
    capacity = max(16, 2 * rows * top_count // experts)
    slots = peers * capacity
    pool_width = w_out.shape[0]
    wide, tile = width // CHUNKS, 256
    tail_width = groups * channels + 256
    vmem = pl.BlockSpec(memory_space=pltpu.VMEM)
    hbm = pl.BlockSpec(memory_space=pl.ANY)
    exchange = pltpu.VMEM((2, CHUNKS, peers, capacity, wide), BF16)
    dma = pltpu.SemaphoreType.DMA
    return pl.pallas_call(
        functools.partial(layer_kernel, sp_count, tp_count),
        out_shape=jax.ShapeDtypeStruct(residual.shape, BF16),
        in_specs=[vmem] * 9 + [hbm] * 5,
        out_specs=vmem,
        scratch_shapes=[
            pltpu.VMEM((1, tail_width), F32),
            pltpu.VMEM((sp_count, 1, tail_width), F32),
            pltpu.VMEM((groups, channels, length), BF16),
            pltpu.VMEM((groups, channels, length), BF16),
            pltpu.VMEM((tp_count, groups, channels, rows), BF16),
            pltpu.VMEM((tp_count, groups, channels, rows), BF16),
            pltpu.VMEM((rows, width), BF16),
            pltpu.VMEM((rows, width), BF16),
            pltpu.VMEM((rows, pool_width), BF16),
            pltpu.VMEM((rows, pool_width), BF16),
            pltpu.VMEM((top_count, rows), jnp.int32),
            pltpu.VMEM((top_count, rows), F32),
            pltpu.VMEM((pool_width, width), BF16),
            pltpu.VMEM((width, hidden_width), BF16),
            pltpu.VMEM((width, hidden_width), BF16),
            pltpu.VMEM((hidden_width, width), BF16),
            pltpu.VMEM((rows, width), BF16),
            pltpu.VMEM((CHUNKS, rows, wide), BF16),
            pltpu.VMEM((2, slots, rows), BF16),
            pltpu.VMEM((2, rows, slots), BF16),
            pltpu.VMEM((2, rows, slots), BF16),
            exchange,
            exchange,
            pltpu.VMEM((hidden_width // tile, slots, tile), BF16),
            exchange,
            exchange,
            pltpu.VMEM((CHUNKS, rows, wide), F32),
            pltpu.VMEM((CHUNKS, rows, wide), BF16),
            pltpu.VMEM((CHUNKS, rows, wide), BF16),
            dma((5,)),
            dma((sp_count,)),
            dma((sp_count,)),
            dma((groups,)),
            dma((groups,)),
            dma((tp_count,)),
            dma((tp_count,)),
            dma((PIECES + 3,)),
            dma((PIECES + 3,)),
            dma((2, CHUNKS)),
            dma((2, CHUNKS)),
            dma((2, CHUNKS)),
            dma((2, CHUNKS)),
            dma((CHUNKS,)),
            dma((CHUNKS,)),
        ],
        compiler_params=pltpu.CompilerParams(
            collective_id=0, has_side_effects=True, vmem_limit_bytes=67043328
        ),
    )(
        pool_input,
        doc_ids.reshape(1, -1),
        pool_map,
        pool_scale.reshape(1, -1),
        mix_gain.reshape(1, -1),
        ffn_gain.reshape(1, -1),
        out_gain.reshape(1, -1),
        expert_ids.T,
        route_logits.T,
        residual,
        w_out,
        w_gate,
        w_up,
        w_down,
    )


def solution(mesh):
    rows = P(("sp", "tp"), None)
    cubes = P(("sp", "tp"), None, None)
    in_specs = (
        P(None, "tp", "sp"), P("sp"), P(), P(), P(), rows, P(), P(), P(), rows, rows,
        cubes, cubes, cubes,
    )
    return jax.shard_map(local, mesh=mesh, in_specs=in_specs, out_specs=rows, check_vma=False)
```

time: 252 us -> 204 us (0.81)
  Pallas kernels: 27.1 us -> 198 us
  blocking collectives: 96.2 us -> 0 us
  waiting for transfers between devices: 93.2 us -> 0 us
  matrix products: 26.1 us -> 0 us
  starting transfers between devices: 3.93 us -> 0 us
  other arithmetic: 3.48 us -> 0 us
    pallas_call x1, Pallas kernels: 27.1 us -> 198 us  [local(): pl.pallas_call(functools.partial(layer_kernel, sp_count, tp_count), out_s...]
    all_to_all x1 -> x0, blocking collectives: 96.2 us -> none  [local(): lax.all_to_all(outgoing, ('sp', 'tp'), split_axis=0, concat_axis=0, tiled...]
    all_to_all x1 -> x0, waiting for transfers between devices: 93.2 us -> none  [local(): lax.all_to_all(finished, ('sp', 'tp'), split_axis=0, concat_axis=0, tiled...]
    dot_general x7 -> x0, matrix products: 26.1 us -> none  [the longest x1 6.1 us: expert_rows(): jnp.dot(hidden, w_down[0], preferred_element_type=jnp.float32)]
    all_to_all x1 -> x0, starting transfers between devices: 3.93 us -> none  [local(): lax.all_to_all(finished, ('sp', 'tp'), split_axis=0, concat_axis=0, tiled...]
  transfers between devices with their start and end apart: 1 -> 0, of which waited for: 1 -> 0; matrix products, arithmetic and copies ran while one was open for 0% -> 0% of each run, Pallas kernels for 0% -> 0%
where the time goes in v1:
time: 204 us; the launch traced here: 200 us
  Pallas kernels  198 us (97%)
  local copies, waits for them, and re-layouts  2.3 us (1%)
    pallas_call x1, Pallas kernels, local(): pl.pallas_call(functools.partial(layer_kernel, sp_count, tp_count), out_s...  198 us

profile of v1, /device:TPU:4, one launch (start us, length us, event | category | flops | bytes accessed | tf_op | source)
XLA Modules:
  0.0 200.2 jit_solution(16400719183656490978)
XLA Ops:
  0.0 197.9 %shard_map.136 = bf16[256,2048]{1,0:T(8,128)(2,1)} custom-call(bf16[4,64,512]{2,1,0:T(8,128)(2,1)} %pool_ref.1, s32[1,512]{1,0:T(1,128)} %bitcast.10, bf16[4,128,128]{2,1,0:T(8,128)(2,1)} %map_ref.1, f32[1,512]{1,0:T(1,128)} %bitcast.11, f32[1,2048]{1,0:T(1,128)} %bitcast.7, f32[1,2048]{1,0:T(1,128)} %bitcast.8, f32[1,2048]{1,0:T(1,128)} %bitcast.9, ...), custom_call_target="tpu_custom_call" | custom-call | tf_op jit(solution)/shard_map/pallas_call | solution.py:387
  197.9 2.3 %copy.16 = bf16[256,2048]{1,0:T(8,128)(2,1)} copy(bf16[256,2048]{1,0:T(8,128)(2,1)} %shard_map.136) | data formatting | bytes 2097152

commit v2 on v1

v2 whole, which is shorter than its diff:
```python
import functools
import jax
import jax.numpy as jnp
from jax import lax
from jax.sharding import PartitionSpec as P
from jax.experimental import pallas as pl
from jax.experimental.pallas import tpu as pltpu

MESH = pl.DeviceIdType.MESH
EPS = 1e-06
CHUNKS = 4
PLANES = 4
F32 = jnp.float32
BF16 = jnp.bfloat16


def rms_scale(vector):
    return lax.rsqrt(jnp.mean(vector * vector, axis=-1, keepdims=True) + EPS)


def contract(left, right, left_dim, right_dim, **options):
    return lax.dot_general(
        left, right, (((left_dim,), (right_dim,)), ((), ())), preferred_element_type=F32, **options
    )


VISITS = ((0, 1, 2, 3), (1, 0, 2, 3), (2, 3, 1, 0), (3, 2, 1, 0))


def layer_kernel(
    sp_count, tp_count,
    pool_ref, doc_ref, map_ref, scale_ref, mix_ref, ffn_ref, gain_ref, ids_ref, logits_ref,
    residual_hbm, w_out_hbm, w_gate_hbm, w_up_hbm, w_down_hbm,
    out_ref,
    tail_out, tails, run_out, far, diff_out, parts, route_own, routes,
    resid, mapped, w_out, w_gate, w_up, w_down,
    stream, normed, picked, mix_high, mix_low,
    outgoing, arrived, hidden, finished, results, total, partial_out, partial_in,
    load_sem, tail_send, tail_recv, far_send, far_recv, diff_send, diff_recv,
    route_send, route_recv, up_send, down_send, line_recv,
    out_send, out_recv, back_send, back_recv, part_send, part_recv,
):
    groups, channels, length = pool_ref.shape
    rows = length // tp_count
    lines = groups * channels
    chunks, wide = normed.shape[1], normed.shape[3]
    peers, capacity = outgoing.shape[2], outgoing.shape[3]
    slots = peers * capacity
    depth, _, tile = hidden.shape
    sp, tp = lax.axis_index("sp"), lax.axis_index("tp")
    plane_size = sp_count // PLANES
    plane = sp // plane_size
    spot = sp - plane * plane_size
    me = spot * tp_count + tp
    last = PLANES - 1
    low, high = plane == 0, plane == last
    visits = [
        sum((plane == q).astype(jnp.int32) * s for q, s in enumerate(column))
        for column in zip(*VISITS)
    ]

    def in_line(other):
        return (other * plane_size + spot, tp)

    loads = []
    for i, (source, target) in enumerate((
        (residual_hbm, resid), (w_out_hbm, w_out), (w_gate_hbm.at[0], w_gate),
        (w_up_hbm.at[0], w_up), (w_down_hbm.at[0], w_down),
    )):
        copy = pltpu.make_async_copy(source, target, load_sem.at[i])
        copy.start()
        loads.append(copy)

    barrier = pltpu.get_barrier_semaphore()
    for i in range(1, sp_count):
        pl.semaphore_signal(
            barrier, inc=1, device_id=(lax.rem(sp + i, sp_count), tp), device_id_type=MESH
        )
    for j in range(plane_size):
        for i in range(1, tp_count):
            pl.semaphore_signal(
                barrier, inc=1,
                device_id=(plane * plane_size + j, lax.rem(tp + i, tp_count)),
                device_id_type=MESH,
            )

    values = pool_ref[...].reshape(lines, length)
    doc = doc_ref[...].astype(F32)
    last_id = doc[:, length - 1 :]
    tail_mask = jnp.broadcast_to((doc == last_id).astype(BF16), (8, length))
    tail_sum = contract(tail_mask, values, 1, 1)[:1]
    tail_count = jnp.sum((doc == last_id).astype(F32), axis=1, keepdims=True)
    tail_row = jnp.concatenate(
        [
            tail_sum,
            jnp.broadcast_to(last_id, (1, 128)),
            jnp.broadcast_to(tail_count, (1, 128)),
        ],
        axis=1,
    )
    tail_out[...] = tail_row
    tails[sp] = tail_row
    route = jnp.concatenate([ids_ref[...].astype(F32), logits_ref[...]], axis=0)
    route_own[...] = route
    routes[plane] = route
    doc_col = jnp.broadcast_to(doc, (128, length)).T[:, :1]
    row_at = lax.broadcasted_iota(jnp.int32, (length, length), 0)
    col_at = lax.broadcasted_iota(jnp.int32, (length, length), 1)
    same = jnp.where((row_at <= col_at) & (doc_col == doc), 1.0, 0.0)
    local_count = jnp.sum(same, axis=0, keepdims=True)
    local_run = jnp.dot(values, same.astype(BF16), preferred_element_type=F32)
    run_out[...] = local_run.astype(BF16).reshape(groups, channels, length)
    pl.semaphore_wait(barrier, sp_count - 1 + plane_size * (tp_count - 1))

    def send(source, target, send_sem, recv_sem, device):
        copy = pltpu.make_async_remote_copy(
            src_ref=source,
            dst_ref=target,
            send_sem=send_sem,
            recv_sem=recv_sem,
            device_id=device,
            device_id_type=MESH,
        )
        copy.start()
        return copy

    early = [
        send(
            tail_out, tails.at[sp], tail_send.at[i], tail_recv.at[i],
            (lax.rem(sp + i, sp_count), tp),
        )
        for i in range(1, sp_count)
    ]
    early += [
        send(
            run_out.at[g], far.at[g], far_send.at[g], far_recv.at[g],
            (lax.rem(sp + 2**g, sp_count), tp),
        )
        for g in reversed(range(groups))
    ]
    route_copies = [
        send(
            route_own, routes.at[plane], route_send.at[i], route_recv.at[i],
            in_line(lax.rem(plane + i, PLANES)),
        )
        for i in range(1, PLANES)
    ]

    expand = (
        lax.broadcasted_iota(jnp.int32, (slots, peers), 0) // capacity
        == lax.broadcasted_iota(jnp.int32, (slots, peers), 1)
    ).astype(BF16)
    at_row = lax.broadcasted_iota(jnp.int32, (rows, rows), 0)
    at_col = lax.broadcasted_iota(jnp.int32, (rows, rows), 1)
    earlier = (at_row < at_col).astype(BF16)
    slot_down = lax.rem(lax.broadcasted_iota(jnp.int32, (slots, rows), 0), capacity).astype(F32)
    slot_across = lax.rem(lax.broadcasted_iota(jnp.int32, (rows, slots), 1), capacity).astype(F32)
    experts = (lax.broadcasted_iota(jnp.int32, (peers, rows), 0) + plane * peers).astype(F32)

    def place(block):
        route = routes[block]
        first, second = route[0:1] == experts, route[1:2] == experts
        named = jnp.where(first | second, 1.0, 0.0)
        rank = jnp.dot(named.astype(BF16), earlier, preferred_element_type=F32)
        code = jnp.where(named > 0.0, rank, -1.0).astype(BF16)
        picked[block] = jnp.where(
            jnp.dot(expand, code, preferred_element_type=F32) == slot_down, 1.0, 0.0
        ).astype(BF16)
        weight = jnp.where(first, jax.nn.sigmoid(route[2:3] - route[3:4]), 0.0) + jnp.where(
            second, jax.nn.sigmoid(route[3:4] - route[2:3]), 0.0
        )
        top = weight.astype(BF16)
        rest = (weight - top.astype(F32)).astype(BF16)
        here = contract(code, expand, 0, 1) == slot_across
        mix_high[block] = jnp.where(here, contract(top, expand, 0, 1), 0.0).astype(BF16)
        mix_low[block] = jnp.where(here, contract(rest, expand, 0, 1), 0.0).astype(BF16)

    for copy in early:
        copy.wait()
    table = jnp.concatenate([tails[j] for j in range(sp_count)], axis=0)
    sources = lax.broadcasted_iota(jnp.int32, (sp_count, 1), 0)
    joined = jnp.where((sources < sp) & (table[:, lines : lines + 1] == doc), 1.0, 0.0)
    position = local_count + jnp.sum(
        joined * table[:, lines + 128 : lines + 129], axis=0, keepdims=True
    )
    for g in range(groups):
        span = float(length * 2**g)
        at = slice(g * channels, (g + 1) * channels)
        between = contract(
            table[:, at], jnp.where(sources >= sp - 2**g, joined, 0.0), 0, 0,
            precision=lax.Precision.HIGHEST,
        )
        window = local_run[at] + between - jnp.where(position > span, far[g].astype(F32), 0.0)
        diff = window / jnp.minimum(position, span) - values[at].astype(F32)
        diff = diff.astype(BF16)
        for q in range(tp_count):
            diff_out[q, g] = diff[:, q * rows : (q + 1) * rows]
    parts[tp] = diff_out[tp]
    diff_copies = []
    for i in range(1, tp_count):
        other = lax.rem(tp + i, tp_count)
        diff_copies.append(
            send(diff_out.at[other], parts.at[tp], diff_send.at[i], diff_recv.at[i], (sp, other))
        )
    place(plane)
    loads[0].wait()
    loads[1].wait()
    for copy in diff_copies:
        copy.wait()
    for g in range(groups):
        channel_rows = jnp.concatenate([parts[q, g] for q in range(tp_count)], axis=0)
        size = tp_count * channels
        at = slice(g * size, (g + 1) * size)
        mapped[:, at] = (contract(channel_rows, map_ref[g], 0, 0) * scale_ref[:, at]).astype(BF16)

    step = min(rows, 128)

    def norm_rows(i, carry):
        at = pl.ds(pl.multiple_of(i * step, step), step)
        projected = jnp.dot(mapped[at, :], w_out[...], preferred_element_type=F32)
        line = (
            resid[at, :].astype(F32) + mix_ref[...] * projected * rms_scale(projected)
        ).astype(BF16)
        stream[at, :] = line
        back = line.astype(F32)
        ready = (ffn_ref[...] * back * rms_scale(back)).astype(BF16)
        for c in range(chunks):
            normed[plane, c, at, :] = ready[:, c * wide : (c + 1) * wide]
        return carry

    lax.fori_loop(0, rows // step, norm_rows, 0)

    def pass_on(s, c, upward, wait):
        target = plane + 1 if upward else plane - 1
        copy = pltpu.make_async_remote_copy(
            src_ref=normed.at[s, c],
            dst_ref=normed.at[s, c],
            send_sem=(up_send if upward else down_send).at[s, c],
            recv_sem=line_recv.at[s, c],
            device_id=in_line(target),
            device_id_type=MESH,
        )
        if wait:
            copy.wait_send()
        else:
            copy.start()

    def pass_both(s, c, wait=False):
        @pl.when((s <= plane) & (plane < last))
        def _():
            pass_on(s, c, True, wait)

        @pl.when((s >= plane) & (plane > 0))
        def _():
            pass_on(s, c, False, wait)

    def spread(source, target, send_sem, recv_sem, k, c):
        def body(i, carry):
            peer = lax.rem(me + i, peers)
            pltpu.make_async_remote_copy(
                src_ref=source.at[k, c, peer],
                dst_ref=target.at[k, c, me],
                send_sem=send_sem.at[k, c],
                recv_sem=recv_sem.at[k, c],
                device_id=(plane * plane_size + peer // tp_count, lax.rem(peer, tp_count)),
                device_id_type=MESH,
            ).start()
            return carry

        lax.fori_loop(1, peers, body, 0)
        target[k, c, me] = source[k, c, me]

    def settle(buffer, sem, k, c):
        whole = buffer.at[k, c, pl.ds(0, peers - 1)]
        pltpu.make_async_copy(whole, whole, sem.at[k, c]).wait()

    def every(body, first=0, end=4):
        def wrapped(c, carry):
            body(c)
            return carry

        lax.fori_loop(chunks * first // 4, chunks * end // 4, wrapped, 0)

    def hand_out(k, c):
        s = visits[k]
        if k > 0:
            pltpu.make_async_copy(normed.at[s, c], normed.at[s, c], line_recv.at[s, c]).wait()
            pass_both(s, c)
        packed = jnp.dot(picked[s], normed[s, c], preferred_element_type=F32)
        outgoing[k, c] = packed.astype(BF16).reshape(peers, capacity, wide)
        spread(outgoing, arrived, out_send, out_recv, k, c)

    def give_out(k, c):
        spread(finished, results, back_send, back_recv, k, c)

    def run_expert(k, give):
        every(lambda c: settle(arrived, out_recv, k, c))

        def body(f, carry):
            at = pl.ds(pl.multiple_of(f * tile, tile), tile)
            gate = jnp.zeros((slots, tile), F32)
            up = jnp.zeros((slots, tile), F32)
            for c in range(chunks):
                line = arrived[k, c].reshape(slots, wide)
                inner = slice(c * wide, (c + 1) * wide)
                gate = gate + jnp.dot(line, w_gate[inner, at], preferred_element_type=F32)
                up = up + jnp.dot(line, w_up[inner, at], preferred_element_type=F32)
            hidden[f] = (jax.nn.silu(gate) * up).astype(BF16)
            return carry

        lax.fori_loop(0, depth, body, 0)

        def give_back(c):
            at = pl.ds(pl.multiple_of(c * wide, wide), wide)
            value = jnp.zeros((slots, wide), F32)
            for f in range(depth):
                inner = slice(f * tile, (f + 1) * tile)
                value = value + jnp.dot(hidden[f], w_down[inner, at], preferred_element_type=F32)
            finished[k, c] = value.astype(BF16).reshape(peers, capacity, wide)
            if give:
                give_out(k, c)

        every(give_back)

    def gathered(k, c):
        s = visits[k]
        settle(results, back_recv, k, c)
        line = results[k, c].reshape(slots, wide)
        return jnp.dot(mix_high[s], line, preferred_element_type=F32) + jnp.dot(
            mix_low[s], line, preferred_element_type=F32
        )

    def part_copy(k, c):
        s = visits[k]
        target = jnp.where(s > plane, plane + 1, plane - 1)
        slot = jnp.where(s == plane - 1, PLANES, s)
        return pltpu.make_async_remote_copy(
            src_ref=partial_out.at[s, c],
            dst_ref=partial_in.at[slot, c],
            send_sem=part_send.at[s, c],
            recv_sem=part_recv.at[slot, c],
            device_id=in_line(target),
            device_id_type=MESH,
        )

    def await_part(slot, c):
        ref = partial_in.at[slot, c]
        pltpu.make_async_copy(ref, ref, part_recv.at[slot, c]).wait()

    def give_end(k, c):
        partial_out[visits[k], c] = gathered(k, c).astype(BF16)
        part_copy(k, c).start()

    def give_middle(k, c):
        s = visits[k]
        value = gathered(k, c)
        await_part(s, c)
        partial_out[s, c] = (value + partial_in[s, c].astype(F32)).astype(BF16)
        part_copy(k, c).start()

    def hand(k, first=0, end=4):
        every(lambda c: hand_out(k, c), first, end)

    def part(k, first=0, end=4):
        every(lambda c: give_end(k, c), first, end)

    def own(c):
        total[c] = gathered(0, c)

    every(lambda c: pass_both(plane, c))
    hand(0)
    for copy in route_copies:
        copy.wait()
    for k in range(1, PLANES):
        place(visits[k])
    for copy in loads[2:]:
        copy.wait()

    @pl.when(low | high)
    def _():
        hand(1)
        run_expert(0, False)
        run_expert(1, True)
        hand(2, 0, 2)
        part(1, 0, 2)
        hand(2, 2, 3)
        part(1, 2, 3)
        hand(2, 3, 4)
        part(1, 3, 4)
        run_expert(2, True)
        hand(3, 0, 2)
        part(2, 0, 2)
        hand(3, 2, 3)
        part(2, 2, 3)
        hand(3, 3, 4)
        part(2, 3, 4)
        run_expert(3, True)
        every(lambda c: give_out(0, c))
        part(3)
        every(own)

    @pl.when(jnp.logical_not(low | high))
    def _():
        def both_in(c):
            hand_out(1, c)
            hand_out(2, c)

        every(both_in)
        run_expert(0, False)
        hand(3, 0, 1)
        run_expert(1, False)
        hand(3, 1, 2)
        run_expert(2, True)
        hand(3, 2, 4)
        every(lambda c: give_out(1, c))
        run_expert(3, True)
        every(lambda c: give_out(0, c))
        every(lambda c: give_middle(2, c))

        def both_out(c):
            give_middle(3, c)
            give_middle(1, c)

        every(both_out)
        every(own)

    @pl.when(plane > 0)
    def _():
        def body(c):
            await_part(plane, c)
            total[c] = total[c] + partial_in[plane, c].astype(F32)

        every(body)

    @pl.when(plane < last)
    def _():
        def body(c):
            await_part(PLANES, c)
            total[c] = total[c] + partial_in[PLANES, c].astype(F32)

        every(body)

    def finish(i, carry):
        at = pl.ds(pl.multiple_of(i * step, step), step)
        summed = jnp.concatenate([total[c, at, :] for c in range(chunks)], axis=1)
        out_ref[at, :] = (
            stream[at, :].astype(F32) + gain_ref[...] * summed * rms_scale(summed)
        ).astype(BF16)
        return carry

    lax.fori_loop(0, rows // step, finish, 0)
    for k in range(PLANES):
        every(lambda c: settle(outgoing, out_send, k, c))
        every(lambda c: settle(finished, back_send, k, c))
        every(lambda c: pass_both(visits[k], c, True))
        if k > 0:
            every(lambda c: part_copy(k, c).wait_send())


def local(
    pool_input, doc_ids, pool_map, pool_scale, w_out, residual, mix_gain, ffn_gain, out_gain,
    expert_ids, route_logits, w_gate, w_up, w_down,
):
    groups, channels, length = pool_input.shape
    sp_count, tp_count = lax.axis_size("sp"), lax.axis_size("tp")
    rows, top_count = expert_ids.shape
    width, hidden_width = w_gate.shape[1], w_gate.shape[2]
    experts = sp_count * tp_count
    peers = experts // PLANES
    capacity = max(16, 2 * rows * top_count // experts)
    slots = peers * capacity
    pool_width = w_out.shape[0]
    wide, tile = width // CHUNKS, 256
    tail_width = groups * channels + 256
    vmem = pl.BlockSpec(memory_space=pltpu.VMEM)
    hbm = pl.BlockSpec(memory_space=pl.ANY)
    exchange = pltpu.VMEM((PLANES, CHUNKS, peers, capacity, wide), BF16)
    dma = pltpu.SemaphoreType.DMA
    each = dma((PLANES, CHUNKS))
    return pl.pallas_call(
        functools.partial(layer_kernel, sp_count, tp_count),
        out_shape=jax.ShapeDtypeStruct(residual.shape, BF16),
        in_specs=[vmem] * 9 + [hbm] * 5,
        out_specs=vmem,
        scratch_shapes=[
            pltpu.VMEM((1, tail_width), F32),
            pltpu.VMEM((sp_count, 1, tail_width), F32),
            pltpu.VMEM((groups, channels, length), BF16),
            pltpu.VMEM((groups, channels, length), BF16),
            pltpu.VMEM((tp_count, groups, channels, rows), BF16),
            pltpu.VMEM((tp_count, groups, channels, rows), BF16),
            pltpu.VMEM((2 * top_count, rows), F32),
            pltpu.VMEM((PLANES, 2 * top_count, rows), F32),
            pltpu.VMEM((rows, width), BF16),
            pltpu.VMEM((rows, pool_width), BF16),
            pltpu.VMEM((pool_width, width), BF16),
            pltpu.VMEM((width, hidden_width), BF16),
            pltpu.VMEM((width, hidden_width), BF16),
            pltpu.VMEM((hidden_width, width), BF16),
            pltpu.VMEM((rows, width), BF16),
            pltpu.VMEM((PLANES, CHUNKS, rows, wide), BF16),
            pltpu.VMEM((PLANES, slots, rows), BF16),
            pltpu.VMEM((PLANES, rows, slots), BF16),
            pltpu.VMEM((PLANES, rows, slots), BF16),
            exchange,
            exchange,
            pltpu.VMEM((hidden_width // tile, slots, tile), BF16),
            exchange,
            exchange,
            pltpu.VMEM((CHUNKS, rows, wide), F32),
            pltpu.VMEM((PLANES, CHUNKS, rows, wide), BF16),
            pltpu.VMEM((PLANES + 1, CHUNKS, rows, wide), BF16),
            dma((5,)),
            dma((sp_count,)),
            dma((sp_count,)),
            dma((groups,)),
            dma((groups,)),
            dma((tp_count,)),
            dma((tp_count,)),
            dma((PLANES,)),
            dma((PLANES,)),
            each,
            each,
            each,
            each,
            each,
            each,
            each,
            each,
            dma((PLANES + 1, CHUNKS)),
        ],
        compiler_params=pltpu.CompilerParams(
            collective_id=0, has_side_effects=True, vmem_limit_bytes=67043328
        ),
    )(
        pool_input,
        doc_ids.reshape(1, -1),
        pool_map,
        pool_scale.reshape(1, -1),
        mix_gain.reshape(1, -1),
        ffn_gain.reshape(1, -1),
        out_gain.reshape(1, -1),
        expert_ids.T,
        route_logits.T,
        residual,
        w_out,
        w_gate,
        w_up,
        w_down,
    )


def solution(mesh):
    rows = P(("sp", "tp"), None)
    cubes = P(("sp", "tp"), None, None)
    in_specs = (
        P(None, "tp", "sp"), P("sp"), P(), P(), P(), rows, P(), P(), P(), rows, rows,
        cubes, cubes, cubes,
    )
    return jax.shard_map(local, mesh=mesh, in_specs=in_specs, out_specs=rows, check_vma=False)
```

time: 204 us -> 164 us (0.80); the launches traced: 200 us -> 164 us
  Pallas kernels: 198 us -> 161 us
    pallas_call x1, Pallas kernels: 198 us -> 161 us  [local(): pl.pallas_call(functools.partial(layer_kernel, sp_count, tp_count), out_s...]
where the time goes in v2:
time: 164 us
  Pallas kernels  161 us (98%)
  local copies, waits for them, and re-layouts  2.3 us (1%)
    pallas_call x1, Pallas kernels, local(): pl.pallas_call(functools.partial(layer_kernel, sp_count, tp_count), out_s...  161 us

profile of v2, /device:TPU:4, one launch (start us, length us, event | category | flops | bytes accessed | tf_op | source)
XLA Modules:
  0.0 163.6 jit_solution(4072680124068574994)
XLA Ops:
  0.0 161.3 %shard_map.136 = bf16[256,2048]{1,0:T(8,128)(2,1)} custom-call(bf16[4,64,512]{2,1,0:T(8,128)(2,1)} %pool_ref.1, s32[1,512]{1,0:T(1,128)} %bitcast.10, bf16[4,128,128]{2,1,0:T(8,128)(2,1)} %map_ref.1, f32[1,512]{1,0:T(1,128)} %bitcast.11, f32[1,2048]{1,0:T(1,128)} %bitcast.7, f32[1,2048]{1,0:T(1,128)} %bitcast.8, f32[1,2048]{1,0:T(1,128)} %bitcast.9, ...), custom_call_target="tpu_custom_call" | custom-call | tf_op jit(solution)/shard_map/pallas_call | solution.py:480
  161.3 2.3 %copy.16 = bf16[256,2048]{1,0:T(8,128)(2,1)} copy(bf16[256,2048]{1,0:T(8,128)(2,1)} %shard_map.136) | data formatting | bytes 2097152

commit v3 on v2

v3 whole, which is shorter than its diff:
```python
import functools
import jax
import jax.numpy as jnp
from jax import lax
from jax.sharding import PartitionSpec as P
from jax.experimental import pallas as pl
from jax.experimental.pallas import tpu as pltpu

MESH = pl.DeviceIdType.MESH
EPS = 1e-06
CHUNKS = 4
PLANES = 4
F32 = jnp.float32
BF16 = jnp.bfloat16


def rms_scale(vector):
    return lax.rsqrt(jnp.mean(vector * vector, axis=-1, keepdims=True) + EPS)


def contract(left, right, left_dim, right_dim, **options):
    return lax.dot_general(
        left, right, (((left_dim,), (right_dim,)), ((), ())), preferred_element_type=F32, **options
    )


VISITS = ((0, 2, 3, 1), (1, 0, 2, 3), (2, 3, 1, 0), (3, 1, 0, 2))


def remote(source, target, send_sem, recv_sem, device):
    return pltpu.make_async_remote_copy(
        src_ref=source,
        dst_ref=target,
        send_sem=send_sem,
        recv_sem=recv_sem,
        device_id=device,
        device_id_type=MESH,
    )


def send(*copy):
    made = remote(*copy)
    made.start()
    return made


def mixer_kernel(
    sp_count, tp_count,
    pool_ref, doc_ref, map_ref, scale_ref, mix_ref, ffn_ref, ids_ref, logits_ref,
    residual_hbm, w_out_hbm,
    stream, normed, routes, most,
    tail_out, tails, run_out, far, diff_out, parts, route_own, most_out, most_in,
    resid, mapped, w_out,
    load_sem, tail_send, tail_recv, far_send, far_recv, diff_send, diff_recv,
    most_send, most_recv, route_send, route_recv,
):
    groups, channels, length = pool_ref.shape
    rows = length // tp_count
    lines = groups * channels
    chunks, _, wide = normed.shape
    sp, tp = lax.axis_index("sp"), lax.axis_index("tp")
    plane_size = sp_count // PLANES
    peers = plane_size * tp_count
    plane = sp // plane_size
    spot = sp - plane * plane_size
    last = PLANES - 1

    loads = []
    for i, (source, target) in enumerate(((residual_hbm, resid), (w_out_hbm, w_out))):
        copy = pltpu.make_async_copy(source, target, load_sem.at[i])
        copy.start()
        loads.append(copy)

    barrier = pltpu.get_barrier_semaphore()
    for i in range(1, sp_count):
        pl.semaphore_signal(
            barrier, inc=1, device_id=(lax.rem(sp + i, sp_count), tp), device_id_type=MESH
        )
    for i in range(1, tp_count):
        pl.semaphore_signal(
            barrier, inc=1, device_id=(sp, lax.rem(tp + i, tp_count)), device_id_type=MESH
        )

    route = jnp.concatenate([ids_ref[...].astype(F32), logits_ref[...]], axis=0)
    route_own[...] = route
    routes[plane] = route
    count = jnp.zeros((1, 1), F32)
    for edge in (0, last):
        bound = jnp.where(plane == edge, 0.0, jnp.sum(needed(route, edge, peers), axis=1, keepdims=True))
        count = jnp.maximum(count, bound)
    values = pool_ref[...].reshape(lines, length)
    doc = doc_ref[...].astype(F32)
    last_id = doc[:, length - 1 :]
    tail_mask = jnp.broadcast_to((doc == last_id).astype(BF16), (8, length))
    tail_sum = contract(tail_mask, values, 1, 1)[:1]
    tail_count = jnp.sum((doc == last_id).astype(F32), axis=1, keepdims=True)
    tail_row = jnp.concatenate(
        [
            tail_sum,
            jnp.broadcast_to(last_id, (1, 128)),
            jnp.broadcast_to(tail_count, (1, 128)),
            jnp.broadcast_to(count, (1, 128)),
        ],
        axis=1,
    )
    tail_out[...] = tail_row
    tails[sp] = tail_row
    doc_col = jnp.broadcast_to(doc, (128, length)).T[:, :1]
    row_at = lax.broadcasted_iota(jnp.int32, (length, length), 0)
    col_at = lax.broadcasted_iota(jnp.int32, (length, length), 1)
    same = jnp.where((row_at <= col_at) & (doc_col == doc), 1.0, 0.0)
    local_count = jnp.sum(same, axis=0, keepdims=True)
    local_run = jnp.dot(values, same.astype(BF16), preferred_element_type=F32)
    run_out[...] = local_run.astype(BF16).reshape(groups, channels, length)
    pl.semaphore_wait(barrier, sp_count + tp_count - 2)
    early = [
        send(
            tail_out, tails.at[sp], tail_send.at[i], tail_recv.at[i],
            (lax.rem(sp + i, sp_count), tp),
        )
        for i in range(1, sp_count)
    ]
    early += [
        send(
            run_out.at[g], far.at[g], far_send.at[g], far_recv.at[g],
            (lax.rem(sp + 2**g, sp_count), tp),
        )
        for g in reversed(range(groups))
    ]
    route_copies = [
        send(
            route_own, routes.at[plane], route_send.at[i], route_recv.at[i],
            (lax.rem(plane + i, PLANES) * plane_size + spot, tp),
        )
        for i in range(1, PLANES)
    ]

    for copy in early:
        copy.wait()
    table = jnp.concatenate([tails[j] for j in range(sp_count)], axis=0)
    sources = lax.broadcasted_iota(jnp.int32, (sp_count, 1), 0)
    joined = jnp.where((sources < sp) & (table[:, lines : lines + 1] == doc), 1.0, 0.0)
    position = local_count + jnp.sum(
        joined * table[:, lines + 128 : lines + 129], axis=0, keepdims=True
    )
    for g in range(groups):
        span = float(length * 2**g)
        at = slice(g * channels, (g + 1) * channels)
        between = contract(
            table[:, at], jnp.where(sources >= sp - 2**g, joined, 0.0), 0, 0,
            precision=lax.Precision.HIGHEST,
        )
        window = local_run[at] + between - jnp.where(position > span, far[g].astype(F32), 0.0)
        diff = window / jnp.minimum(position, span) - values[at].astype(F32)
        diff = diff.astype(BF16)
        for q in range(tp_count):
            diff_out[q, g] = diff[:, q * rows : (q + 1) * rows]
    parts[tp] = diff_out[tp]
    most_out[...] = jnp.broadcast_to(
        jnp.max(table[:, lines + 256 : lines + 257], axis=0, keepdims=True), (1, 128)
    )
    most_in[tp] = most_out[...]
    diff_copies = []
    for i in range(1, tp_count):
        other = lax.rem(tp + i, tp_count)
        diff_copies.append(
            send(diff_out.at[other], parts.at[tp], diff_send.at[i], diff_recv.at[i], (sp, other))
        )
        diff_copies.append(
            send(most_out, most_in.at[tp], most_send.at[i], most_recv.at[i], (sp, other))
        )
    loads[0].wait()
    loads[1].wait()
    for copy in diff_copies:
        copy.wait()
    for g in range(groups):
        channel_rows = jnp.concatenate([parts[q, g] for q in range(tp_count)], axis=0)
        size = tp_count * channels
        at = slice(g * size, (g + 1) * size)
        mapped[:, at] = (contract(channel_rows, map_ref[g], 0, 0) * scale_ref[:, at]).astype(BF16)

    step = min(rows, 128)

    def norm_rows(i, carry):
        at = pl.ds(pl.multiple_of(i * step, step), step)
        projected = jnp.dot(mapped[at, :], w_out[...], preferred_element_type=F32)
        line = (
            resid[at, :].astype(F32) + mix_ref[...] * projected * rms_scale(projected)
        ).astype(BF16)
        stream[at, :] = line
        back = line.astype(F32)
        ready = (ffn_ref[...] * back * rms_scale(back)).astype(BF16)
        for c in range(chunks):
            normed[c, at, :] = ready[:, c * wide : (c + 1) * wide]
        return carry

    lax.fori_loop(0, rows // step, norm_rows, 0)

    top = most_in[0]
    for q in range(1, tp_count):
        top = jnp.maximum(top, most_in[q])
    most[...] = top.astype(jnp.int32)
    for copy in route_copies:
        copy.wait()


def needed(route, edge, peers):
    first, second = route[0:1], route[1:2]
    low, high = edge * peers, (edge + 1) * peers
    if not isinstance(edge, int):
        low, high = low.astype(F32), high.astype(F32)
    return jnp.where(
        ((first >= low) & (first < high)) | ((second >= low) & (second < high)), 1.0, 0.0
    )


def layer_kernel(
    sp_count, tp_count,
    normed_own, routes, gain_ref, stream_hbm, w_gate_hbm, w_up_hbm, w_down_hbm,
    out_ref,
    stream, w_gate, w_up, w_down,
    normed, picked, mix_high, mix_low, packs, forward,
    outgoing, arrived, hidden, results, total, partial_out, partial_in,
    load_sem, near_send, edge_send, line_recv,
    out_send, out_recv, back_send, back_recv, part_send, part_recv,
):
    chunks, rows, wide = normed_own.shape
    peers, capacity = outgoing.shape[2], outgoing.shape[3]
    slots = peers * capacity
    packed = packs.shape[1]
    depth, _, tile = hidden.shape
    sp, tp = lax.axis_index("sp"), lax.axis_index("tp")
    plane_size = sp_count // PLANES
    plane = sp // plane_size
    spot = sp - plane * plane_size
    me = spot * tp_count + tp
    last = PLANES - 1
    outer = (plane == 0) | (plane == last)
    edge = jnp.where(plane <= 1, 0, last)
    inner = jnp.where(plane <= 1, 1 + plane, plane - 1)
    visits = [
        sum((plane == q).astype(jnp.int32) * s for q, s in enumerate(column))
        for column in zip(*VISITS)
    ]

    def in_line(other):
        return (other * plane_size + spot, tp)

    loads = []
    for i, (source, target) in enumerate((
        (w_gate_hbm.at[0], w_gate), (w_up_hbm.at[0], w_up), (w_down_hbm.at[0], w_down),
        (stream_hbm, stream),
    )):
        copy = pltpu.make_async_copy(source, target, load_sem.at[i])
        copy.start()
        loads.append(copy)

    barrier = pltpu.get_barrier_semaphore()
    for i in range(1, PLANES):
        pl.semaphore_signal(
            barrier, inc=1, device_id=in_line(lax.rem(plane + i, PLANES)), device_id_type=MESH
        )
    for i in range(1, peers):
        peer = lax.rem(me + i, peers)
        pl.semaphore_signal(
            barrier, inc=1,
            device_id=(plane * plane_size + peer // tp_count, lax.rem(peer, tp_count)),
            device_id_type=MESH,
        )

    expand = (
        lax.broadcasted_iota(jnp.int32, (slots, peers), 0) // capacity
        == lax.broadcasted_iota(jnp.int32, (slots, peers), 1)
    ).astype(BF16)
    at_row = lax.broadcasted_iota(jnp.int32, (rows, rows), 0)
    at_col = lax.broadcasted_iota(jnp.int32, (rows, rows), 1)
    earlier = (at_row < at_col).astype(BF16)
    slot_down = lax.rem(lax.broadcasted_iota(jnp.int32, (slots, rows), 0), capacity).astype(F32)
    slot_across = lax.rem(lax.broadcasted_iota(jnp.int32, (rows, slots), 1), capacity).astype(F32)
    experts = (lax.broadcasted_iota(jnp.int32, (peers, rows), 0) + plane * peers).astype(F32)

    pack_down = lax.broadcasted_iota(jnp.int32, (packed, rows), 0).astype(F32)

    def place(block, compact, forwarded):
        route = routes[block]
        first, second = route[0:1] == experts, route[1:2] == experts
        named = jnp.where(first | second, 1.0, 0.0)
        rank = jnp.dot(named.astype(BF16), earlier, preferred_element_type=F32)
        code = jnp.where(named > 0.0, rank, -1.0).astype(BF16)
        chosen = jnp.where(
            jnp.dot(expand, code, preferred_element_type=F32) == slot_down, 1.0, 0.0
        ).astype(BF16)
        weight = jnp.where(first, jax.nn.sigmoid(route[2:3] - route[3:4]), 0.0) + jnp.where(
            second, jax.nn.sigmoid(route[3:4] - route[2:3]), 0.0
        )
        top = weight.astype(BF16)
        rest = (weight - top.astype(F32)).astype(BF16)
        here = contract(code, expand, 0, 1) == slot_across
        top = jnp.where(here, contract(top, expand, 0, 1), 0.0).astype(BF16)
        rest = jnp.where(here, contract(rest, expand, 0, 1), 0.0).astype(BF16)
        if compact or forwarded:
            need = jnp.broadcast_to(needed(route, edge, peers), (8, rows))
            turn = jnp.dot(need.astype(BF16), earlier, preferred_element_type=F32)
            turn = jnp.where(need > 0.0, turn, -1.0)[0:1]
            pack = jnp.where(turn == pack_down, 1.0, 0.0).astype(BF16)
            if forwarded:
                packs[block] = pack
        if compact:
            picked[block, :, 0:packed] = contract(chosen, pack, 1, 1).astype(BF16)
            mix_high[block, 0:packed] = jnp.dot(pack, top, preferred_element_type=F32).astype(BF16)
            mix_low[block, 0:packed] = jnp.dot(pack, rest, preferred_element_type=F32).astype(BF16)
        else:
            picked[block] = chosen
            mix_high[block] = top
            mix_low[block] = rest

    def to_inner(k, c):
        s = visits[k]
        source = normed_own.at[c] if k == 0 else normed.at[s, c]
        return remote(
            source, normed.at[s, c], near_send.at[k, c], line_recv.at[s, c], in_line(inner)
        )

    def to_edge(k, c):
        s = visits[k]
        return remote(
            forward.at[k, c], normed.at[s, c, pl.ds(0, packed)],
            edge_send.at[k, c], line_recv.at[s, c], in_line(edge),
        )

    def pack_edge(k, c):
        s = visits[k]
        source = normed_own[c] if k == 0 else normed[s, c]
        forward[k, c] = jnp.dot(packs[s], source, preferred_element_type=F32).astype(BF16)
        to_edge(k, c).start()

    def spread(source, target, send_sem, recv_sem, k, c):
        def body(i, carry):
            peer = lax.rem(me + i, peers)
            pltpu.make_async_remote_copy(
                src_ref=source.at[k, c, peer],
                dst_ref=target.at[k, c, me],
                send_sem=send_sem.at[k, c],
                recv_sem=recv_sem.at[k, c],
                device_id=(plane * plane_size + peer // tp_count, lax.rem(peer, tp_count)),
                device_id_type=MESH,
            ).start()
            return carry

        lax.fori_loop(1, peers, body, 0)
        target[k, c, me] = source[k, c, me]

    def settle(buffer, sem, k, c):
        whole = buffer.at[k, c, pl.ds(0, peers - 1)]
        pltpu.make_async_copy(whole, whole, sem.at[k, c]).wait()

    def every(body, first=0, end=4):
        def wrapped(c, carry):
            body(c)
            return carry

        lax.fori_loop(chunks * first // 4, chunks * end // 4, wrapped, 0)

    def fetch(k, c, height):
        ref = normed.at[visits[k], c, pl.ds(0, height)]
        pltpu.make_async_copy(ref, ref, line_recv.at[visits[k], c]).wait()

    def hand_out(k, c, height):
        s = visits[k]
        source = normed_own[c] if k == 0 else normed[s, c, 0:height]
        value = jnp.dot(picked[s, :, 0:height], source, preferred_element_type=F32)
        outgoing[k, c] = value.astype(BF16).reshape(peers, capacity, wide)
        spread(outgoing, arrived, out_send, out_recv, k, c)

    def give_out(k, c):
        spread(outgoing, results, back_send, back_recv, k, c)

    def run_expert(k, give):
        every(lambda c: settle(arrived, out_recv, k, c))

        def body(f, carry):
            at = pl.ds(pl.multiple_of(f * tile, tile), tile)
            gate = jnp.zeros((slots, tile), F32)
            up = jnp.zeros((slots, tile), F32)
            for c in range(chunks):
                line = arrived[k, c].reshape(slots, wide)
                inner = slice(c * wide, (c + 1) * wide)
                gate = gate + jnp.dot(line, w_gate[inner, at], preferred_element_type=F32)
                up = up + jnp.dot(line, w_up[inner, at], preferred_element_type=F32)
            hidden[f] = (jax.nn.silu(gate) * up).astype(BF16)
            return carry

        lax.fori_loop(0, depth, body, 0)

        def give_back(c):
            at = pl.ds(pl.multiple_of(c * wide, wide), wide)
            value = jnp.zeros((slots, wide), F32)
            for f in range(depth):
                inner = slice(f * tile, (f + 1) * tile)
                value = value + jnp.dot(hidden[f], w_down[inner, at], preferred_element_type=F32)
            settle(outgoing, out_send, k, c)
            outgoing[k, c] = value.astype(BF16).reshape(peers, capacity, wide)
            if give:
                give_out(k, c)

        every(give_back)

    def gathered(k, c, height):
        s = visits[k]
        settle(results, back_recv, k, c)
        line = results[k, c].reshape(slots, wide)
        return jnp.dot(mix_high[s, 0:height], line, preferred_element_type=F32) + jnp.dot(
            mix_low[s, 0:height], line, preferred_element_type=F32
        )

    def part_copy(k, c, height, target):
        s = visits[k]
        slot = jnp.where((s == target) & (target < plane), PLANES, s)
        at = pl.ds(0, height)
        return remote(
            partial_out.at[s, c, at], partial_in.at[slot, c, at],
            part_send.at[s, c], part_recv.at[slot, c], in_line(target),
        )

    def await_part(slot, c, height):
        ref = partial_in.at[slot, c, pl.ds(0, height)]
        pltpu.make_async_copy(ref, ref, part_recv.at[slot, c]).wait()

    def unpacked(s, slot, c):
        await_part(slot, c, packed)
        return contract(packs[s], partial_in[slot, c, 0:packed], 0, 0)

    def give_end(k, c):
        partial_out[visits[k], c, 0:packed] = gathered(k, c, packed).astype(BF16)
        part_copy(k, c, packed, inner).start()

    def give_far(k, c):
        s = visits[k]
        value = gathered(k, c, rows) + unpacked(s, s, c)
        partial_out[s, c] = value.astype(BF16)
        part_copy(k, c, rows, inner).start()

    def give_near(k, c):
        s = visits[k]
        value = gathered(k, c, rows)
        await_part(s, c, rows)
        partial_out[s, c] = (value + partial_in[s, c].astype(F32)).astype(BF16)
        part_copy(k, c, rows, edge).start()

    def own(c):
        total[c] = gathered(0, c, rows)

    def out_of(k, first=0, end=4):
        every(lambda c: give_out(k, c), first, end)

    def drain():
        for k in range(PLANES):
            every(lambda c: settle(outgoing, back_send, k, c))

    place(plane, False, True)
    pl.semaphore_wait(barrier, PLANES + peers - 2)

    @pl.when(outer)
    def _():
        def hand(k, first=0, end=4):
            def body(c):
                fetch(k, c, packed)
                hand_out(k, c, packed)

            every(body, first, end)

        def part(k, first=0, end=4):
            every(lambda c: give_end(k, c), first, end)

        every(lambda c: to_inner(0, c).start())
        every(lambda c: hand_out(0, c, rows))
        for k in range(1, PLANES):
            place(visits[k], True, False)
        for copy in loads[:3]:
            copy.wait()
        hand(1, 0, 1)
        run_expert(0, False)
        out_of(0, 0, 1)
        hand(1, 1, 2)
        out_of(0, 1, 2)
        hand(1, 2, 4)
        run_expert(1, True)
        hand(2, 0, 2)
        part(1, 0, 2)
        hand(2, 2, 3)
        part(1, 2, 4)
        hand(2, 3, 4)
        hand(3, 0, 2)
        run_expert(2, True)
        hand(3, 2, 4)
        part(2)
        run_expert(3, True)
        out_of(0, 2, 4)
        part(3)
        every(own)
        home = jnp.where(plane == 0, PLANES, plane)

        def finish(c):
            await_part(home, c, rows)
            total[c] = total[c] + partial_in[home, c].astype(F32)

        every(finish)
        every(lambda c: to_inner(0, c).wait_send())
        for k in range(1, PLANES):
            every(lambda c: part_copy(k, c, packed, inner).wait_send())

    @pl.when(jnp.logical_not(outer))
    def _():
        def hand_far(first, end):
            def body(c):
                fetch(3, c, rows)
                pack_edge(3, c)
                hand_out(3, c, rows)

            every(body, first, end)

        def both_in(c):
            fetch(2, c, rows)
            pack_edge(2, c)
            fetch(1, c, rows)
            to_inner(1, c).start()
            hand_out(2, c, rows)
            hand_out(1, c, rows)

        every(lambda c: to_inner(0, c).start())
        every(lambda c: pack_edge(0, c), 0, 2)
        every(lambda c: hand_out(0, c, rows), 0, 2)
        for k in range(1, PLANES):
            place(visits[k], False, k > 1)
        for copy in loads[:3]:
            copy.wait()
        every(both_in)
        hand_far(0, 1)
        run_expert(2, True)
        hand_far(1, 3)
        run_expert(1, False)
        hand_far(3, 4)
        every(lambda c: pack_edge(0, c), 2, 4)
        every(lambda c: hand_out(0, c, rows), 2, 4)
        out_of(1)
        every(lambda c: give_far(2, c))
        run_expert(3, True)
        run_expert(0, False)
        out_of(0)
        every(lambda c: give_far(3, c), 0, 2)
        every(lambda c: give_near(1, c), 0, 1)
        every(lambda c: give_far(3, c), 2, 3)
        every(lambda c: give_near(1, c), 1, 2)
        every(lambda c: give_far(3, c), 3, 4)
        every(lambda c: give_near(1, c), 2, 4)
        every(own)
        far_slot = jnp.where(edge == 0, plane, PLANES)
        near_slot = jnp.where(edge == 0, PLANES, plane)

        def finish(c):
            value = total[c] + unpacked(plane, far_slot, c)
            await_part(near_slot, c, rows)
            total[c] = value + partial_in[near_slot, c].astype(F32)

        every(finish)
        for k in (0, 1):
            every(lambda c: to_inner(k, c).wait_send())
        for k in (0, 2, 3):
            every(lambda c: to_edge(k, c).wait_send())
        for k in (2, 3):
            every(lambda c: part_copy(k, c, rows, inner).wait_send())
        every(lambda c: part_copy(1, c, rows, edge).wait_send())

    loads[3].wait()
    step = min(rows, 128)

    def finish(i, carry):
        at = pl.ds(pl.multiple_of(i * step, step), step)
        summed = jnp.concatenate([total[c, at, :] for c in range(chunks)], axis=1)
        out_ref[at, :] = (
            stream[at, :].astype(F32) + gain_ref[...] * summed * rms_scale(summed)
        ).astype(BF16)
        return carry

    lax.fori_loop(0, rows // step, finish, 0)
    drain()


def mixer(
    pool_input, doc_ids, pool_map, pool_scale, w_out, residual, mix_gain, ffn_gain,
    expert_ids, route_logits,
):
    groups, channels, length = pool_input.shape
    sp_count, tp_count = lax.axis_size("sp"), lax.axis_size("tp")
    rows, width = residual.shape
    top_count = expert_ids.shape[1]
    pool_width = w_out.shape[0]
    wide = width // CHUNKS
    tail_width = groups * channels + 384
    vmem = pl.BlockSpec(memory_space=pltpu.VMEM)
    hbm = pl.BlockSpec(memory_space=pl.ANY)
    dma = pltpu.SemaphoreType.DMA
    return pl.pallas_call(
        functools.partial(mixer_kernel, sp_count, tp_count),
        out_shape=(
            jax.ShapeDtypeStruct((rows, width), BF16),
            jax.ShapeDtypeStruct((CHUNKS, rows, wide), BF16),
            jax.ShapeDtypeStruct((PLANES, 2 * top_count, rows), F32),
            jax.ShapeDtypeStruct((1, 128), jnp.int32),
        ),
        in_specs=[vmem] * 8 + [hbm] * 2,
        out_specs=(vmem,) * 4,
        scratch_shapes=[
            pltpu.VMEM((1, tail_width), F32),
            pltpu.VMEM((sp_count, 1, tail_width), F32),
            pltpu.VMEM((groups, channels, length), BF16),
            pltpu.VMEM((groups, channels, length), BF16),
            pltpu.VMEM((tp_count, groups, channels, rows), BF16),
            pltpu.VMEM((tp_count, groups, channels, rows), BF16),
            pltpu.VMEM((2 * top_count, rows), F32),
            pltpu.VMEM((1, 128), F32),
            pltpu.VMEM((tp_count, 1, 128), F32),
            pltpu.VMEM((rows, width), BF16),
            pltpu.VMEM((rows, pool_width), BF16),
            pltpu.VMEM((pool_width, width), BF16),
            dma((2,)),
            dma((sp_count,)),
            dma((sp_count,)),
            dma((groups,)),
            dma((groups,)),
            dma((tp_count,)),
            dma((tp_count,)),
            dma((tp_count,)),
            dma((tp_count,)),
            dma((PLANES,)),
            dma((PLANES,)),
        ],
        compiler_params=pltpu.CompilerParams(
            collective_id=0, has_side_effects=True, vmem_limit_bytes=67043328
        ),
    )(
        pool_input,
        doc_ids.reshape(1, -1),
        pool_map,
        pool_scale.reshape(1, -1),
        mix_gain.reshape(1, -1),
        ffn_gain.reshape(1, -1),
        expert_ids.T,
        route_logits.T,
        residual,
        w_out,
    )


def expert_layer(packed, collective_id, normed, routes, out_gain, stream, w_gate, w_up, w_down):
    sp_count, tp_count = lax.axis_size("sp"), lax.axis_size("tp")
    _, rows, wide = normed.shape
    width, hidden_width = w_gate.shape[1], w_gate.shape[2]
    top_count = routes.shape[1] // 2
    experts = sp_count * tp_count
    peers = experts // PLANES
    capacity = max(16, 2 * rows * top_count // experts)
    slots = peers * capacity
    tile = 256
    vmem = pl.BlockSpec(memory_space=pltpu.VMEM)
    hbm = pl.BlockSpec(memory_space=pl.ANY)
    exchange = pltpu.VMEM((PLANES, CHUNKS, peers, capacity, wide), BF16)
    dma = pltpu.SemaphoreType.DMA
    each = dma((PLANES, CHUNKS))
    return pl.pallas_call(
        functools.partial(layer_kernel, sp_count, tp_count),
        out_shape=jax.ShapeDtypeStruct(stream.shape, BF16),
        in_specs=[vmem] * 3 + [hbm] * 4,
        out_specs=vmem,
        scratch_shapes=[
            pltpu.VMEM((rows, width), BF16),
            pltpu.VMEM((width, hidden_width), BF16),
            pltpu.VMEM((width, hidden_width), BF16),
            pltpu.VMEM((hidden_width, width), BF16),
            pltpu.VMEM((PLANES, CHUNKS, rows, wide), BF16),
            pltpu.VMEM((PLANES, slots, rows), BF16),
            pltpu.VMEM((PLANES, rows, slots), BF16),
            pltpu.VMEM((PLANES, rows, slots), BF16),
            pltpu.VMEM((PLANES, packed, rows), BF16),
            pltpu.VMEM((PLANES, CHUNKS, packed, wide), BF16),
            exchange,
            exchange,
            pltpu.VMEM((hidden_width // tile, slots, tile), BF16),
            exchange,
            pltpu.VMEM((CHUNKS, rows, wide), F32),
            pltpu.VMEM((PLANES, CHUNKS, rows, wide), BF16),
            pltpu.VMEM((PLANES + 1, CHUNKS, rows, wide), BF16),
            dma((4,)),
            each,
            each,
            each,
            each,
            each,
            each,
            each,
            each,
            dma((PLANES + 1, CHUNKS)),
        ],
        compiler_params=pltpu.CompilerParams(
            collective_id=collective_id, has_side_effects=True, vmem_limit_bytes=67043328
        ),
    )(normed, routes, out_gain.reshape(1, -1), stream, w_gate, w_up, w_down)


def local(
    pool_input, doc_ids, pool_map, pool_scale, w_out, residual, mix_gain, ffn_gain, out_gain,
    expert_ids, route_logits, w_gate, w_up, w_down,
):
    stream, normed, routes, most = mixer(
        pool_input, doc_ids, pool_map, pool_scale, w_out, residual, mix_gain, ffn_gain,
        expert_ids, route_logits,
    )
    rows = residual.shape[0]
    packed = 3 * rows // 4
    operands = (normed, routes, out_gain, stream, w_gate, w_up, w_down)
    return lax.cond(
        most[0, 0] <= packed,
        functools.partial(expert_layer, packed, 1),
        functools.partial(expert_layer, rows, 2),
        *operands,
    )


def solution(mesh):
    rows = P(("sp", "tp"), None)
    cubes = P(("sp", "tp"), None, None)
    in_specs = (
        P(None, "tp", "sp"), P("sp"), P(), P(), P(), rows, P(), P(), P(), rows, rows,
        cubes, cubes, cubes,
    )
    return jax.shard_map(local, mesh=mesh, in_specs=in_specs, out_specs=rows, check_vma=False)
```

time: 164 us -> 147 us (0.90); the launches traced: 164 us -> 145 us
  Pallas kernels: 161 us -> 142 us
    pallas_call x1 -> x2, Pallas kernels: 161 us -> 142 us  [the longest x1 118 us: expert_layer(): pl.pallas_call(functools.partial(layer_kernel, sp_count, tp_count), out_s...]
where the time goes in v3:
time: 147 us; the launch traced here: 145 us
  Pallas kernels  142 us (97%)
  local copies, waits for them, and re-layouts  2.3 us (2%)
    pallas_call x1, Pallas kernels, expert_layer(): pl.pallas_call(functools.partial(layer_kernel, sp_count, tp_count), out_s...  118 us
    pallas_call x1, Pallas kernels, mixer(): pl.pallas_call(functools.partial(mixer_kernel, sp_count, tp_count), out_s...  23.4 us

profile of v3, /device:TPU:4, one launch (start us, length us, event | category | flops | bytes accessed | tf_op | source)
XLA Modules:
  0.0 144.9 jit_solution(3761744212003387553)
XLA Ops:
  0.0 23.4 %shard_map.138 = (bf16[256,2048]{1,0:T(8,128)(2,1)}, bf16[4,256,512]{2,1,0:T(8,128)(2,1)}, f32[4,4,256]{2,1,0:T(4,128)}, s32[1,128]{1,0:T(1,128)}) custom-call(bf16[4,64,512]{2,1,0:T(8,128)(2,1)} %pool_ref.1, s32[1,512]{1,0:T(1,128)} %bitcast.14, bf16[4,128,128]{2,1,0:T(8,128)(2,1)} %map_ref.1, f32[1,512]{1,0:T(1,128)} %bitcast.15, f32[1,2048]{1,0:T(1,128)} %bitcast.12, ...), custom_call_target="tpu_custom_call" | custom-call | tf_op jit(solution)/shard_map/pallas_call | solution.py:603
  23.9 118.7 %conditional.1 = (bf16[256,2048]{1,0:T(8,128)(2,1)}) conditional(s32[]{:T(128)} %bitcast.8, (f32[2048]{0:T(1024)}, bf16[4,256,512]{2,1,0:T(8,128)(2,1)}, f32[4,4,256]{2,1,0:T(4,128)}, bf16[256,2048]{1,0:T(8,128)(2,1)}, bf16[1,2048,1024]{2,1,0:T(8,128)(2,1)}, /*index=5*/bf16[1,2048,1024]{2,1,0:T(8,128)(2,1)}, ...), branch_computations={%region_0.0_spmd, %region_1.0_spmd} | conditional | bytes 8 | solution.py:721
  24.1 118.2 %branch_1_fun.1 = bf16[256,2048]{1,0:T(8,128)(2,1)} custom-call(bf16[4,256,512]{2,1,0:T(8,128)(2,1)} %get-tuple-element.43.normed_own, f32[4,4,256]{2,1,0:T(4,128)} %get-tuple-element.44.routes, f32[1,2048]{1,0:T(1,128)} %bitcast.11, bf16[256,2048]{1,0:T(8,128)(2,1)} %get-tuple-element.46.stream_hbm, bf16[1,2048,1024]{2,1,0:T(8,128)(2,1)} %get-tuple-element.47.w_gate_hbm, ...), custom_call_target="tpu_custom_call" | custom-call | tf_op jit(solution)/shard_map/cond/branch_1_fun/pallas_call | solution.py:670
  142.6 2.3 %copy.20 = bf16[256,2048]{1,0:T(8,128)(2,1)} copy(bf16[256,2048]{1,0:T(8,128)(2,1)} %get-tuple-element.58) | data formatting | bytes 2097152

commit v4 on v3

--- a/solution.py
+++ b/solution.py
@@ -220,7 +220,7 @@
     out_ref,
     stream, w_gate, w_up, w_down,
     normed, picked, mix_high, mix_low, packs, forward,
-    outgoing, arrived, hidden, results, total, partial_out, partial_in,
+    outgoing, arrived, gate_sum, up_sum, hidden, results, total, partial_out, partial_in,
     load_sem, near_send, edge_send, line_recv,
     out_send, out_recv, back_send, back_recv, part_send, part_recv,
 ):
@@ -375,7 +375,7 @@
     def give_out(k, c):
         spread(outgoing, results, back_send, back_recv, k, c)
 
-    def run_expert(k, give):
+    def first_half(k):
         every(lambda c: settle(arrived, out_recv, k, c))
 
         def body(f, carry):
@@ -391,6 +391,39 @@
             return carry
 
         lax.fori_loop(0, depth, body, 0)
+
+    def first_half_by_chunk(k):
+        gate_sum[...] = jnp.zeros_like(gate_sum)
+        up_sum[...] = jnp.zeros_like(up_sum)
+
+        def take(c, finish):
+            settle(arrived, out_recv, k, c)
+            inner = pl.ds(pl.multiple_of(c * wide, wide), wide)
+
+            def body(f, carry):
+                at = pl.ds(pl.multiple_of(f * tile, tile), tile)
+                line = arrived[k, c].reshape(slots, wide)
+                gate = gate_sum[f] + jnp.dot(
+                    line, w_gate[inner, at], preferred_element_type=F32
+                )
+                up = up_sum[f] + jnp.dot(line, w_up[inner, at], preferred_element_type=F32)
+                if finish:
+                    hidden[f] = (jax.nn.silu(gate) * up).astype(BF16)
+                else:
+                    gate_sum[f] = gate
+                    up_sum[f] = up
+                return carry
+
+            lax.fori_loop(0, depth, body, 0)
+
+        every(lambda c: take(c, False), 0, 3)
+        take(chunks - 1, True)
+
+    def run_expert(k, give, by_chunk=False):
+        if by_chunk:
+            first_half_by_chunk(k)
+        else:
+            first_half(k)
 
         def give_back(c):
             at = pl.ds(pl.multiple_of(c * wide, wide), wide)
@@ -484,17 +517,17 @@
         hand(1, 1, 2)
         out_of(0, 1, 2)
         hand(1, 2, 4)
-        run_expert(1, True)
+        run_expert(1, True, True)
         hand(2, 0, 2)
         part(1, 0, 2)
         hand(2, 2, 3)
         part(1, 2, 4)
         hand(2, 3, 4)
         hand(3, 0, 2)
-        run_expert(2, True)
+        run_expert(2, True, True)
         hand(3, 2, 4)
         part(2)
-        run_expert(3, True)
+        run_expert(3, True, True)
         out_of(0, 2, 4)
         part(3)
         every(own)
@@ -685,6 +718,8 @@
             pltpu.VMEM((PLANES, CHUNKS, packed, wide), BF16),
             exchange,
             exchange,
+            pltpu.VMEM((hidden_width // tile, slots, tile), F32),
+            pltpu.VMEM((hidden_width // tile, slots, tile), F32),
             pltpu.VMEM((hidden_width // tile, slots, tile), BF16),
             exchange,
             pltpu.VMEM((CHUNKS, rows, wide), F32),

time: 147 us -> 143 us (0.973)
  Pallas kernels: 142 us -> 139 us
    pallas_call x1, Pallas kernels: 118 us -> 115 us  [expert_layer(): pl.pallas_call(functools.partial(layer_kernel, sp_count, tp_count), out_s...]
where the time goes in v4:
time: 143 us; the launch traced here: 142 us
  Pallas kernels  139 us (97%)
  local copies, waits for them, and re-layouts  2.3 us (2%)
    pallas_call x1, Pallas kernels, expert_layer(): pl.pallas_call(functools.partial(layer_kernel, sp_count, tp_count), out_s...  115 us
    pallas_call x1, Pallas kernels, mixer(): pl.pallas_call(functools.partial(mixer_kernel, sp_count, tp_count), out_s...  23.4 us

profile of v4, /device:TPU:4, one launch (start us, length us, event | category | flops | bytes accessed | tf_op | source)
XLA Modules:
  0.0 142.0 jit_solution(5682525192352114010)
XLA Ops:
  0.0 23.4 %shard_map.138 = (bf16[256,2048]{1,0:T(8,128)(2,1)}, bf16[4,256,512]{2,1,0:T(8,128)(2,1)}, f32[4,4,256]{2,1,0:T(4,128)}, s32[1,128]{1,0:T(1,128)}) custom-call(bf16[4,64,512]{2,1,0:T(8,128)(2,1)} %pool_ref.1, s32[1,512]{1,0:T(1,128)} %bitcast.14, bf16[4,128,128]{2,1,0:T(8,128)(2,1)} %map_ref.1, f32[1,512]{1,0:T(1,128)} %bitcast.15, f32[1,2048]{1,0:T(1,128)} %bitcast.12, ...), custom_call_target="tpu_custom_call" | custom-call | tf_op jit(solution)/shard_map/pallas_call | solution.py:636
  23.9 115.8 %conditional.1 = (bf16[256,2048]{1,0:T(8,128)(2,1)}) conditional(s32[]{:T(128)} %bitcast.8, (f32[2048]{0:T(1024)}, bf16[4,256,512]{2,1,0:T(8,128)(2,1)}, f32[4,4,256]{2,1,0:T(4,128)}, bf16[256,2048]{1,0:T(8,128)(2,1)}, bf16[1,2048,1024]{2,1,0:T(8,128)(2,1)}, /*index=5*/bf16[1,2048,1024]{2,1,0:T(8,128)(2,1)}, ...), branch_computations={%region_0.0_spmd, %region_1.0_spmd} | conditional | bytes 8 | solution.py:756
  24.1 115.3 %branch_1_fun.1 = bf16[256,2048]{1,0:T(8,128)(2,1)} custom-call(bf16[4,256,512]{2,1,0:T(8,128)(2,1)} %get-tuple-element.43.normed_own, f32[4,4,256]{2,1,0:T(4,128)} %get-tuple-element.44.routes, f32[1,2048]{1,0:T(1,128)} %bitcast.11, bf16[256,2048]{1,0:T(8,128)(2,1)} %get-tuple-element.46.stream_hbm, bf16[1,2048,1024]{2,1,0:T(8,128)(2,1)} %get-tuple-element.47.w_gate_hbm, ...), custom_call_target="tpu_custom_call" | custom-call | tf_op jit(solution)/shard_map/cond/branch_1_fun/pallas_call | solution.py:703
  139.7 2.3 %copy.20 = bf16[256,2048]{1,0:T(8,128)(2,1)} copy(bf16[256,2048]{1,0:T(8,128)(2,1)} %get-tuple-element.58) | data formatting | bytes 2097152
